TPU v7x, 32 devices: a whole 2x2x4 slice. The times are simulated.
32 devices in a mesh: sp: 8 (over z, y), tp: 4 (over x, core).
Axes of the slice: x: 2, y: 2, z: 4, core: 2. Of those that a mesh axis runs over, the one named last changes fastest.
Arguments:
- residual: bfloat16 [2048, 2048], P(('sp', 'tp')), may hold values from -6 to 6
- output_gate_projected: bfloat16 [2048, 4096], P('sp', 'tp'), may hold values from -6 to 6
- value_projected_input: bfloat16 [2048, 4096], P('sp', 'tp'), may hold values from -6 to 6
- state_projected_input: bfloat16 [2048, 2048], P('sp', 'tp'), may hold values from -6 to 6
- readout_projected_input: bfloat16 [2048, 2048], P('sp', 'tp'), may hold values from -6 to 6
- step_preactivation: float32 [2048, 64], P('sp', 'tp'), may hold values from -5 to 5
- position_decay_extra: float32 [2048, 64], P('sp', 'tp')
- value_conv_kernel: bfloat16 [4, 4096], P(None, 'tp'), may hold values from -0.29882812 to 0.29882812
- state_conv_kernel: bfloat16 [4, 2048], P(None, 'tp'), may hold values from -0.8984375 to 0.8984375
- readout_conv_kernel: bfloat16 [4, 2048], P(None, 'tp'), may hold values from -0.8984375 to 0.8984375
- head_log_decay_rates: float32 [64], P('tp')
- head_direct_weight: float32 [64], P('tp'), may hold values from 0.5 to 4
- head_norm_gain: float32 [4096], P('tp'), may hold values from 0.1 to 1.9
- mixer_output_weight: bfloat16 [4096, 2048], P('tp'), may hold values from -0.09375 to 0.09375
- expert_norm_gain: float32 [2048], replicated, may hold values from 0.1 to 1.9
- routed_expert_index: int32 [2048, 4], P(('sp', 'tp')), may hold values from 0 to 7, all different within a row; in each aligned block of 64 rows (0 to 63, 64 to 127, ...) at most 64 rows name the same one
- routed_expert_weight: float32 [2048, 4], P(('sp', 'tp')), may hold values from 0.2 to 1
- routed_gate_weight: bfloat16 [8, 2048, 256], P('sp'), may hold values from -0.125 to 0.125
- routed_up_weight: bfloat16 [8, 2048, 256], P('sp'), may hold values from -0.125 to 0.125
- routed_down_weight: bfloat16 [8, 256, 2048], P('sp'), may hold values from -0.375 to 0.375
- common_gate_weight: bfloat16 [2048, 512], P(None, 'tp'), may hold values from -0.125 to 0.125
- common_up_weight: bfloat16 [2048, 512], P(None, 'tp'), may hold values from -0.125 to 0.125
- common_down_weight: bfloat16 [2048, 512], P(None, 'tp'), may hold values from -0.25 to 0.25
Outputs:
- layer_out: bfloat16 [2048, 2048], P(('sp', 'tp'))
Inputs may be any that keep to these rules, and one draw needn't show every extreme that they name: `routed_expert_index`: among the 64 rows of one device, no expert is named by more than 64 rows.
All inputs are finite; a program needn't handle non-finite values.
Results may differ from a plain program's by a relative error of at most 0.02.
Values may be sent and summed in bfloat16 or wider, within the bound.
A program may use at most 128 MiB of HBM per device.

v0:
```python
import jax
import jax.numpy as jnp
from jax import lax
from jax.sharding import PartitionSpec as P

D = 2048
HEAD_DIM = 64
STATE = 128
CONV = 4
BLOCK_POSITIONS = 128


EPSILON = 1e-06
HIGHEST_PRECISION = lax.Precision.HIGHEST


def shifted(value, axis, steps):
    count = lax.axis_size(axis)
    first, last = (max(0, -steps), min(count, count - steps))
    return lax.ppermute(value, axis, [(source, source + steps) for source in range(first, last)])


def entering(array, axis, combine, identity):
    size, index = (lax.axis_size(axis), lax.axis_index(axis))
    everything = jax.tree.map(
        lambda part, kind: lax.all_gather(part.astype(kind), axis),
        array,
        (jnp.bfloat16, jnp.bfloat16),
    )
    start = jax.tree.map(
        lambda part, zero: jnp.broadcast_to(jnp.asarray(zero, part.dtype), part.shape),
        array,
        identity,
    )

    def hop(k, before):
        reached = k < index
        new = combine(
            before, jax.tree.map(lambda part, own: part[k].astype(own.dtype), everything, array)
        )
        return jax.tree.map(lambda a, b: jnp.where(reached, a, b), new, before)

    return lax.fori_loop(0, size, hop, start)


def short_conv(inputs, rim_rows, weights):
    length = inputs.shape[0]
    extended = jnp.concatenate([rim_rows, inputs], axis=0)
    totals = jnp.zeros(inputs.shape, jnp.float32)
    for tap_index in range(CONV):
        totals = totals + extended[tap_index : tap_index + length].astype(jnp.float32) * weights[
            tap_index
        ].astype(jnp.float32)
    return jax.nn.silu(totals)


def shared_part(rows, gate_piece, up_piece, down_piece):
    gate_part = jnp.dot(rows, gate_piece, preferred_element_type=jnp.float32)
    lifted = jnp.dot(rows, up_piece, preferred_element_type=jnp.float32)
    hidden = (jax.nn.silu(gate_part) * lifted).astype(jnp.bfloat16)
    return jnp.einsum("rc,dc->rd", hidden, down_piece, preferred_element_type=jnp.float32)


def join_states(earlier, later):
    return (earlier[0] * later[0], later[0][..., None, None] * earlier[1] + later[1])


def shards(
    residual,
    output_gate_projected,
    value_projected_input,
    state_projected_input,
    readout_projected_input,
    step_preactivation,
    position_decay_extra,
    value_conv_kernel,
    state_conv_kernel,
    readout_conv_kernel,
    head_log_decay_rates,
    head_direct_weight,
    head_norm_gain,
    mixer_output_weight,
    expert_norm_gain,
    routed_expert_index,
    routed_expert_weight,
    routed_gate_weight,
    routed_up_weight,
    routed_down_weight,
    common_gate_weight,
    common_up_weight,
    common_down_weight,
):
    head_count = step_preactivation.shape[1]
    groups = state_projected_input.shape[1] // STATE
    heads_per_group = head_count // groups
    length = value_projected_input.shape[0]
    block_list = length // BLOCK_POSITIONS
    conv_tails = (
        value_projected_input[length - CONV + 1 :],
        state_projected_input[length - CONV + 1 :],
        readout_projected_input[length - CONV + 1 :],
    )
    value_rim, input_rim, readout_rim = shifted(
        (conv_tails[0], conv_tails[1], conv_tails[2]), "sp", 1
    )
    values = short_conv(value_projected_input, value_rim, value_conv_kernel).reshape(
        block_list, BLOCK_POSITIONS, groups, heads_per_group, HEAD_DIM
    )
    state_in = short_conv(state_projected_input, input_rim, state_conv_kernel).reshape(
        block_list, BLOCK_POSITIONS, groups, STATE
    )
    readout = short_conv(readout_projected_input, readout_rim, readout_conv_kernel).reshape(
        block_list, BLOCK_POSITIONS, groups, STATE
    )
    head_step_lengths = jax.nn.softplus(step_preactivation)
    decay_logarithm = (
        head_step_lengths * (-jnp.exp(head_log_decay_rates))[None, :] + position_decay_extra
    ).reshape(block_list, BLOCK_POSITIONS, groups, heads_per_group)
    head_step_lengths = head_step_lengths.reshape(
        block_list, BLOCK_POSITIONS, groups, heads_per_group
    )
    causal = jnp.arange(BLOCK_POSITIONS)[:, None] >= jnp.arange(BLOCK_POSITIONS)[None, :]
    cumulative = jnp.cumsum(decay_logarithm, axis=1)
    weighted_output = values * head_step_lengths[..., None]
    by_head = jnp.transpose(cumulative, (0, 2, 3, 1))
    span_logs = by_head[..., :, None] - by_head[..., None, :]
    decay_factors = jnp.exp(jnp.where(causal, span_logs, -jnp.inf))
    attention_scores = jnp.einsum("ctgn,csgn->cgts", readout, state_in, precision=HIGHEST_PRECISION)
    within_block_output = jnp.einsum(
        "cgrts,csgrp->ctgrp",
        attention_scores[:, :, None] * decay_factors,
        weighted_output,
        precision=HIGHEST_PRECISION,
    )
    to_end = jnp.exp(cumulative[:, -1:] - cumulative)
    fresh_state = jnp.einsum(
        "csgn,csgrp->cgrpn",
        state_in,
        weighted_output * to_end[..., None],
        precision=HIGHEST_PRECISION,
    )
    block_decay = jnp.exp(cumulative[:, -1])

    def block_chain(carried, block_item):
        state_now, factor = carried
        decay_blk, fresh_blk = block_item
        return (
            (decay_blk[..., None, None] * state_now + fresh_blk, decay_blk * factor),
            (state_now, factor),
        )

    empty_state = jnp.zeros((groups, heads_per_group, HEAD_DIM, STATE), jnp.float32)
    unit_decay = jnp.ones((groups, heads_per_group), jnp.float32)
    (own_state, own_decay), (local_start, local_factor) = lax.scan(
        block_chain, (empty_state, unit_decay), (block_decay, fresh_state)
    )
    incoming = entering((own_decay, own_state), "sp", join_states, (unit_decay, empty_state))
    start_states = local_start + local_factor[..., None, None] * incoming[1][None]
    carried_out = (
        jnp.einsum("ctgn,cgrpn->ctgrp", readout, start_states, precision=HIGHEST_PRECISION)
        * jnp.exp(cumulative)[..., None]
    )
    mixed_heads = (
        within_block_output
        + carried_out
        + head_direct_weight.reshape(groups, heads_per_group)[None, None, :, :, None] * values
    )
    mixed_heads = mixed_heads.reshape(length, head_count, HEAD_DIM) * jax.nn.silu(
        output_gate_projected.reshape(length, head_count, HEAD_DIM).astype(jnp.float32)
    )
    normed = mixed_heads * lax.rsqrt(
        jnp.mean(mixed_heads * mixed_heads, axis=-1, keepdims=True) + EPSILON
    )
    heads_out = (
        (normed * head_norm_gain.reshape(head_count, HEAD_DIM))
        .astype(jnp.bfloat16)
        .reshape(length, head_count * HEAD_DIM)
    )
    row_count = residual.shape[0]
    mix_sum = lax.psum_scatter(
        jnp.dot(heads_out, mixer_output_weight, preferred_element_type=jnp.float32).astype(
            jnp.bfloat16
        ),
        "tp",
        scatter_dimension=0,
        tiled=True,
    ).astype(jnp.float32)
    stream = (residual.astype(jnp.float32) + mix_sum).astype(jnp.bfloat16)
    stream_wide = stream.astype(jnp.float32)
    normed_rows = (
        stream_wide
        * lax.rsqrt(jnp.mean(stream_wide * stream_wide, axis=-1, keepdims=True) + EPSILON)
        * expert_norm_gain
    ).astype(jnp.bfloat16)
    group_rows = lax.all_gather(normed_rows, "tp", axis=0, tiled=True)
    shared = lax.psum_scatter(
        shared_part(group_rows, common_gate_weight, common_up_weight, common_down_weight).astype(
            jnp.bfloat16
        ),
        "tp",
        scatter_dimension=0,
        tiled=True,
    ).astype(jnp.float32)
    local_experts = routed_gate_weight.shape[0]
    experts_all = local_experts * lax.axis_size("sp")
    top_count = routed_expert_index.shape[1]
    capacity = 2 * row_count * top_count // experts_all
    flat_ids = routed_expert_index.reshape(-1)
    expert_hits = (flat_ids[:, None] == jnp.arange(experts_all, dtype=jnp.int32)[None, :]).astype(
        jnp.int32
    )
    slot_ranks = jnp.sum((jnp.cumsum(expert_hits, axis=0) - 1) * expert_hits, axis=1)
    slot_index = flat_ids * capacity + slot_ranks
    slot_rows = (
        jnp.full((experts_all * capacity,), row_count, jnp.int32)
        .at[slot_index]
        .set(jnp.arange(row_count * top_count, dtype=jnp.int32) // top_count)
    )
    padded = jnp.concatenate([normed_rows, jnp.zeros((1, D), jnp.bfloat16)], axis=0)
    outgoing = padded[slot_rows].reshape(experts_all, capacity, D)
    arrived = lax.all_to_all(outgoing, "sp", split_axis=0, concat_axis=0, tiled=True)
    sources = arrived.shape[0] // local_experts
    grouped = arrived.reshape(sources, local_experts, arrived.shape[1], D)
    gate_part = jnp.einsum(
        "sekd,edf->sekf", grouped, routed_gate_weight, preferred_element_type=jnp.float32
    )
    lifted = jnp.einsum(
        "sekd,edf->sekf", grouped, routed_up_weight, preferred_element_type=jnp.float32
    )
    hidden = (jax.nn.silu(gate_part) * lifted).astype(jnp.bfloat16)
    result = jnp.einsum(
        "sekf,efd->sekd", hidden, routed_down_weight, preferred_element_type=jnp.float32
    ).astype(jnp.bfloat16)
    returned = lax.all_to_all(
        result.reshape(arrived.shape), "sp", split_axis=0, concat_axis=0, tiled=True
    )
    picked = returned.reshape(experts_all * capacity, D)[slot_index]
    routed = jnp.sum(
        (picked.astype(jnp.float32) * routed_expert_weight.reshape(-1)[:, None]).reshape(
            row_count, top_count, D
        ),
        axis=1,
    )
    return (stream_wide + shared + routed).astype(jnp.bfloat16)


def solution(mesh):
    placed = (
        P(("sp", "tp"), None),
        P("sp", "tp"),
        P("sp", "tp"),
        P("sp", "tp"),
        P("sp", "tp"),
        P("sp", "tp"),
        P("sp", "tp"),
        P(None, "tp"),
        P(None, "tp"),
        P(None, "tp"),
        P("tp"),
        P("tp"),
        P("tp"),
        P("tp", None),
        P(),
        P(("sp", "tp"), None),
        P(("sp", "tp"), None),
        P("sp", None, None),
        P("sp", None, None),
        P("sp", None, None),
        P(None, "tp"),
        P(None, "tp"),
        P(None, "tp"),
    )
    return jax.shard_map(
        shards, mesh=mesh, in_specs=placed, out_specs=P(("sp", "tp"), None), check_vma=False
    )
```

profile of v0, /device:TPU:0, one launch (start us, length us, event | category | flops | bytes accessed | tf_op | source)
XLA Modules:
  0.0 262.3 jit_solution(18141689269001511208)
XLA Ops:
  6.5 0.8 slice.82
  7.4 0.9 copy.54
  8.2 5.6 %collective-permute-start = (bf16[3,1024]{0,1:T(8,128)(2,1)}, bf16[3,1024]{0,1:T(8,128)(2,1)}, u32[]{:S(2)}, u32[]{:S(2)}) collective-permute-start(bf16[3,1024]{0,1:T(8,128)(2,1)} %copy.54), channel_id=1, source_target_pairs={{0,4},{4,8},{8,12},{12,16},{16,20},{20,24},{24,28},{1,5},{5,9},{9,... | collective-permute-start | bytes 18440 | tf_op jit(solution)/shard_map/ppermute | solution.py:20
  13.9 0.7 slice.98
  14.6 2.7 %collective-permute-start.2 = (bf16[3,512]{1,0:T(4,128)(2,1)S(1)}, bf16[3,512]{1,0:T(4,128)(2,1)S(1)}, u32[]{:S(2)}, u32[]{:S(2)}) collective-permute-start(bf16[3,512]{1,0:T(4,128)(2,1)S(1)} %slice.98), channel_id=1, source_target_pairs={{0,4},{4,8},{8,12},{12,16},{16,20},{20,24},{24,28},{1,5},{5,9},{9,... | collective-permute-start | bytes 9224 | tf_op jit(solution)/shard_map/ppermute | solution.py:20
  17.3 0.9 slice_convert_fusion.3
  18.1 0.7 exponential_negate_fusion
  18.8 0.8 compare_select_fusion
  19.6 0.3 copy.59
  20.1 1.1 fusion.75
  21.2 1.2 copy.55
  22.7 0.3 divide_multiply_fusion.1
  23.1 1.0 reshape.167
  24.0 3.2 %divide_multiply_fusion = f32[256,1024]{0,1:T(8,128)} fusion(bf16[256,1024]{0,1:T(8,128)(2,1)S(1)} %copy.55, bf16[3,1024]{0,1:T(8,128)(2,1)} %collective-permute-done, f32[1024]{0:T(1024)S(1)} %bitcast.153, f32[1024]{0:T(1024)S(1)} %bitcast.154, f32[1024]{0:T(1024)S(1)} %bitcast.152, f32[1024]{0:T(1024)S(1)} %bitcast.151), kind=kLoop, calls=%fused_computation.50 | loop fusion | flops 6291456 | bytes 1595392 | tf_op jit(solution)/shard_map/jit(silu)/mul | solution.py:54
  27.3 1.7 reshape.165
  29.0 1.7 broadcast_multiply_fusion
  30.7 1.1 fusion.27
  31.8 2.1 while.31
  31.9 0.9 bitcast_dynamic-update-slice_fusion.4
  32.9 0.9 bitcast_dynamic-update-slice_fusion.4
  33.9 0.7 convert_element_type.169
  34.7 3.4 %collective-permute-start.1 = (bf16[3,512]{1,0:T(4,128)(2,1)S(1)}, bf16[3,512]{1,0:T(4,128)(2,1)S(1)}, u32[]{:S(2)}, u32[]{:S(2)}) collective-permute-start(bf16[3,512]{1,0:T(4,128)(2,1)S(1)} %slice.90), channel_id=1, source_target_pairs={{0,4},{4,8},{8,12},{12,16},{16,20},{20,24},{24,28},{1,5},{5,9},{9,... | collective-permute-start | bytes 9224 | tf_op jit(solution)/shard_map/ppermute | solution.py:20
  38.2 1.2 copy.67
  39.9 1.5 reshape.191
  41.5 1.1 divide_multiply_fusion.2
  42.6 1.2 reshape.166
  43.8 2.0 fusion.46
  45.9 18.2 %all-gather.2 = bf16[8,4,4]{2,1,0:T(4,128)(2,1)S(1)} all-gather(bf16[1,4,4]{2,1,0:T(4,128)(2,1)S(1)} %convert_bitcast_fusion), channel_id=2, replica_groups=mesh['sp'=8,'tp'=4] {'sp'}, dimensions={0}, use_global_device_ids=true | all-gather | bytes 288 | tf_op jit(solution)/shard_map/all_gather | solution.py:26
  64.0 20.4 %all-gather.8.cloned.1.call-done = bf16[32,4,64,128]{3,2,1,0:T(8,128)(2,1)} async-done(((bf16[4,4,64,128]{3,2,1,0:T(8,128)(2,1)}), bf16[32,4,64,128]{3,2,1,0:T(8,128)(2,1)}) %all-gather.8.cloned.1.call-update) | async-done | bytes 2097168 | tf_op jit(solution)/shard_map/all_gather | solution.py:26
  84.4 9.1 %while.32 = (s32[]{:T(128)}, f32[4,4,64,128]{3,2,1,0:T(8,128)S(1)}, s32[]{:T(128)}, bf16[8,4,4]{2,1,0:T(4,128)(2,1)S(1)}, bf16[8,4,4,64,128]{4,3,2,1,0:T(8,128)(2,1)}, /*index=5*/s32[]{:T(128)}, s32[]{:T(128)}) while((s32[]{:T(128)}, f32[4,4,64,128]{3,2,1,0:T(8,128)S(1)}, s32[]{:T(128)}, bf16[8,4,4]{2,1,0:T(4,128)(2,1)S(1)}, ...), condition=%wide.region_4.5_spmd.clone, body=%wide.region_3.4_spmd.clone.sunk | while | flops 655380 | bytes 1310985 | solution.py:43
  84.4 1.1 fusion.89
  85.6 1.1 fusion.89
  86.7 1.1 fusion.89
  87.9 1.1 fusion.89
  89.0 1.1 fusion.89
  90.1 1.1 fusion.89
  91.2 1.1 fusion.89
  92.4 1.1 fusion.89
  93.5 2.5 fusion.12
  96.1 4.2 %multiply_reduce_fusion.1 = (f32[2,128,4,4]{1,3,2,0:T(4,128)S(1)}, f32[2,128,4,4,64]{1,4,3,2,0:T(8,128)S(1)}) fusion(f32[2,128,4,4,64]{1,0,4,3,2:T(2,128)S(1)} %copy-done.8, f32[2,128,4,4,64]{1,0,4,3,2:T(2,128)S(1)} %copy-done.4, f32[4,4]{1,0:T(4,128)S(1)} %mul.432, f32[2,128,4,4,64]{1,4,3,2,0:T(8,128)S(1)} %fusion.12, f32[2,4,4,128]{3,2,1,0:T(4,128)S(1)} %copy.60, ...), kind=kOutput, calls=%fused_computation.43 | convolution fusion | flops 406843392 | bytes 5816384 | tf_op jit(solution)/shard_map/cgrts,csgrp->ctgrp/dot_general | solution.py:129
  100.4 0.8 copy.69
  101.3 0.4 fusion.22
  101.6 0.9 copy-done.20
  102.6 2.3 convolution_convert_fusion.2
  105.2 0.6 reduce-window.6
  106.4 1.4 scatter_custom_fusion
  107.8 20.5 %reduce-scatter.3.cloned.1.call-done = bf16[64,2048]{1,0:T(8,128)(2,1)} async-done(((bf16[256,2048]{1,0:T(8,128)(2,1)}), bf16[64,2048]{1,0:T(8,128)(2,1)}) %reduce-scatter.3.cloned.1.call-update) | async-done | bytes 262160 | tf_op jit(solution)/shard_map/reduce_scatter | solution.py:180
  128.3 1.1 fusion.37
  129.5 1.1 fusion.39
  130.6 3.3 %gather_fusion = bf16[512,2048]{1,0:T(8,128)(2,1)} fusion(bf16[65,2048]{1,0:T(8,128)(2,1)S(1)} %concatenate.15, s32[1024]{0:T(1024)S(1)} %pad_clamp_fusion.1), kind=kCustom, calls=%fused_computation | custom fusion | bytes 4196352 | tf_op jit(solution)/shard_map/gather | solution.py:220
  133.9 5.5 %all-to-all-start = ((bf16[8,64,2048]{2,1,0:T(8,128)(2,1)}), bf16[8,64,2048]{2,1,0:T(8,128)(2,1)S(1)}, u32[]{:S(2)}, u32[]{:S(2)}) async-start(bf16[8,64,2048]{2,1,0:T(8,128)(2,1)} %bitcast.25), calls=%async_computation.2 | async-start | bytes 4194304 | tf_op jit(solution)/shard_map/all_to_all | solution.py:221
  139.4 0.3 all-gather.6.cloned.1.call-start
  139.7 0.5 all-gather.6.cloned.1.call-update
  140.2 47.3 %all-to-all-done = bf16[8,64,2048]{2,1,0:T(8,128)(2,1)S(1)} async-done(((bf16[8,64,2048]{2,1,0:T(8,128)(2,1)}), bf16[8,64,2048]{2,1,0:T(8,128)(2,1)S(1)}, u32[]{:S(2)}, u32[]{:S(2)}) %all-to-all-start) | async-done | bytes 2097184 | tf_op jit(solution)/shard_map/all_to_all | solution.py:221
  187.5 2.7 %convolution_bitcast_fusion.2 = f32[8,1,64,256]{3,2,0,1:T(8,128)} fusion(bf16[8,64,2048]{2,1,0:T(8,128)(2,1)S(1)} %all-to-all-done, bf16[1,2048,256]{2,1,0:T(8,128)(2,1)} %param.44), kind=kOutput, calls=%fused_computation.26 | convolution fusion | flops 536870912 | bytes 3670016 | tf_op jit(solution)/shard_map/sekd,edf->sekf/dot_general | solution.py:224
  190.3 5.0 %convolution_convert_fusion = bf16[8,64,2048]{2,1,0:T(8,128)(2,1)} fusion(bf16[8,64,2048]{2,1,0:T(8,128)(2,1)S(1)} %all-to-all-done, bf16[1,256,2048]{2,1,0:T(8,128)(2,1)S(1)} %copy-done, bf16[1,2048,256]{2,1,0:T(8,128)(2,1)} %param.45, f32[8,1,64,256]{3,2,0,1:T(8,128)} %convolution_bitcast_fusion.2), kind=kOutput, calls=%fused_computation.11 | convolution fusion | flops 1075576832 | bytes 6815744 | tf_op jit(solution)/shard_map/sekf,efd->sekd/dot_general | solution.py:231
  195.3 3.6 %all-to-all-start.1 = ((bf16[8,64,2048]{2,1,0:T(8,128)(2,1)}), bf16[8,64,2048]{2,1,0:T(8,128)(2,1)S(1)}, u32[]{:S(2)}, u32[]{:S(2)}) async-start(bf16[8,64,2048]{2,1,0:T(8,128)(2,1)} %convolution_convert_fusion), calls=%async_computation.3 | async-start | bytes 4194304 | tf_op jit(solution)/shard_map/all_to_all | solution.py:234
  199.0 1.8 fusion.77
  200.8 3.3 %convolution_convert_fusion.1 = bf16[256,2048]{1,0:T(8,128)(2,1)} fusion(bf16[2048,128]{1,0:T(8,128)(2,1)} %param.49, bf16[256,2048]{1,0:T(8,128)(2,1)} %all-gather.6.cloned.1.call-done, bf16[2048,128]{1,0:T(8,128)(2,1)} %param.48, f32[256,128]{1,0:T(8,128)S(1)} %fusion.77), kind=kOutput, calls=%fused_computation.12 | convolution fusion | flops 269156352 | bytes 3276800 | tf_op jit(solution)/shard_map/rc,dc->rd/dot_general | solution.py:61
  204.2 43.2 %all-to-all-done.1 = bf16[8,64,2048]{2,1,0:T(8,128)(2,1)S(1)} async-done(((bf16[8,64,2048]{2,1,0:T(8,128)(2,1)}), bf16[8,64,2048]{2,1,0:T(8,128)(2,1)S(1)}, u32[]{:S(2)}, u32[]{:S(2)}) %all-to-all-start.1) | async-done | bytes 2097184 | tf_op jit(solution)/shard_map/all_to_all | solution.py:234
  247.3 2.3 gather_fusion.1
  249.7 1.7 reshape.192
  251.4 2.3 multiply_reduce_fusion
  253.7 2.0 fusion.41
  (107 shorter events, 2.6 us)
Async XLA Ops:
  6.5 183.7 %copy-start = (bf16[1,256,2048]{2,1,0:T(8,128)(2,1)S(1)}, bf16[1,256,2048]{2,1,0:T(8,128)(2,1)}, u32[]{:S(2)}) copy-start(bf16[1,256,2048]{2,1,0:T(8,128)(2,1)} %param.46) | copy-start | bytes 3145732
  6.5 14.6 %copy-start.13 = (bf16[4,512]{1,0:T(4,128)(2,1)S(1)}, bf16[4,512]{1,0:T(4,128)(2,1)}, u32[]{:S(2)}) copy-start(bf16[4,512]{1,0:T(4,128)(2,1)} %param.35) | copy-start | bytes 12292
  6.5 77.9 %all-gather.8.cloned.1.call-start = ((), (), s32[]{:S(2)}) async-start(), calls=%async_computation.7 | async-start | bytes 2359296 | tf_op jit(solution)/shard_map/all_gather | solution.py:26
  8.2 15.8 %collective-permute-start = (bf16[3,1024]{0,1:T(8,128)(2,1)}, bf16[3,1024]{0,1:T(8,128)(2,1)}, u32[]{:S(2)}, u32[]{:S(2)}) collective-permute-start(bf16[3,1024]{0,1:T(8,128)(2,1)} %copy.54), channel_id=1, source_target_pairs={{0,4},{4,8},{8,12},{12,16},{16,20},{20,24},{24,28},{1,5},{5,9},{9,... | collective-permute-start | bytes 18440 | tf_op jit(solution)/shard_map/ppermute | solution.py:20
  14.6 8.1 %collective-permute-start.2 = (bf16[3,512]{1,0:T(4,128)(2,1)S(1)}, bf16[3,512]{1,0:T(4,128)(2,1)S(1)}, u32[]{:S(2)}, u32[]{:S(2)}) collective-permute-start(bf16[3,512]{1,0:T(4,128)(2,1)S(1)} %slice.98), channel_id=1, source_target_pairs={{0,4},{4,8},{8,12},{12,16},{16,20},{20,24},{24,28},{1,5},{5,9},{9,... | collective-permute-start | bytes 9224 | tf_op jit(solution)/shard_map/ppermute | solution.py:20
  19.9 2.8 %copy-start.11 = (bf16[256,512]{1,0:T(8,128)(2,1)S(1)}, bf16[256,512]{1,0:T(8,128)(2,1)}, u32[]{:S(2)}) copy-start(bf16[256,512]{1,0:T(8,128)(2,1)} %param.30) | copy-start | bytes 786436
  29.0 1.7 copy-start.3
  29.0 1.7 copy-start.1
  31.8 2.9 %copy-start.12 = (bf16[256,512]{1,0:T(8,128)(2,1)S(1)}, bf16[256,512]{1,0:T(8,128)(2,1)}, u32[]{:S(2)}) copy-start(bf16[256,512]{1,0:T(8,128)(2,1)} %param.31) | copy-start | bytes 786436
  31.8 6.4 %copy-start.14 = (bf16[4,512]{1,0:T(4,128)(2,1)S(1)}, bf16[4,512]{1,0:T(4,128)(2,1)}, u32[]{:S(2)}) copy-start(bf16[4,512]{1,0:T(4,128)(2,1)} %param.36) | copy-start | bytes 12292
  33.9 5.8 %copy-start.10 = (bf16[256,1024]{1,0:T(8,128)(2,1)S(1)}, bf16[256,1024]{1,0:T(8,128)(2,1)}, u32[]{:S(2)}) copy-start(bf16[256,1024]{1,0:T(8,128)(2,1)} %param.28) | copy-start | bytes 1572868
  34.7 6.7 %copy-start.19 = (f32[16]{0:T(128)S(1)}, f32[16]{0:T(128)}, u32[]{:S(2)}) copy-start(f32[16]{0:T(128)} %param.38) | copy-start | bytes 196
  34.7 93.6 %reduce-scatter.3.cloned.1.call-start = ((), (), s32[]{:S(2)}) async-start(), calls=%async_computation.4 | async-start | bytes 1310720 | tf_op jit(solution)/shard_map/reduce_scatter | solution.py:180
  34.7 6.7 %collective-permute-start.1 = (bf16[3,512]{1,0:T(4,128)(2,1)S(1)}, bf16[3,512]{1,0:T(4,128)(2,1)S(1)}, u32[]{:S(2)}, u32[]{:S(2)}) collective-permute-start(bf16[3,512]{1,0:T(4,128)(2,1)S(1)} %slice.90), channel_id=1, source_target_pairs={{0,4},{4,8},{8,12},{12,16},{16,20},{20,24},{24,28},{1,5},{5,9},{9,... | collective-permute-start | bytes 9224 | tf_op jit(solution)/shard_map/ppermute | solution.py:20
  39.7 4.2 %copy-start.2 = (f32[2,128,4,128]{3,2,1,0:T(4,128)S(1)}, f32[2,128,4,128]{3,2,1,0:T(4,128)}, u32[]{:S(2)}) copy-start(f32[2,128,4,128]{3,2,1,0:T(4,128)} %reshape.167) | copy-start | bytes 1572868
  84.4 11.7 %copy-start.9 = (f32[2,4,128,128]{3,2,1,0:T(8,128)S(1)}, f32[2,4,128,128]{3,2,1,0:T(8,128)}, u32[]{:S(2)}) copy-start(f32[2,4,128,128]{3,2,1,0:T(8,128)} %fusion.46) | copy-start | bytes 1572868
  93.5 2.6 copy-start.4
  93.5 2.6 copy-start.7
  93.5 2.6 copy-start.8
  100.4 0.9 copy-start.17
  100.4 2.2 copy-start.20
  102.6 2.3 copy-start.16
  102.6 25.7 %copy-start.5 = (bf16[64,2048]{1,0:T(8,128)(2,1)S(1)}, bf16[64,2048]{1,0:T(8,128)(2,1)}, u32[]{:S(2)}) copy-start(bf16[64,2048]{1,0:T(8,128)(2,1)} %param.27) | copy-start | bytes 786436
  102.6 26.9 %copy-start.15 = (f32[2048]{0:T(1024)S(1)}, f32[2048]{0:T(1024)}, u32[]{:S(2)}) copy-start(f32[2048]{0:T(1024)} %param.41) | copy-start | bytes 24580
  130.5 3.4 %copy-start.6 = (bf16[64,2048]{1,0:T(8,128)(2,1)}, bf16[64,2048]{1,0:T(8,128)(2,1)S(1)}, u32[]{:S(2)}) copy-start(bf16[64,2048]{1,0:T(8,128)(2,1)S(1)} %fusion.39) | copy-start | bytes 786436
  133.9 53.6 %all-to-all-start = ((bf16[8,64,2048]{2,1,0:T(8,128)(2,1)}), bf16[8,64,2048]{2,1,0:T(8,128)(2,1)S(1)}, u32[]{:S(2)}, u32[]{:S(2)}) async-start(bf16[8,64,2048]{2,1,0:T(8,128)(2,1)} %bitcast.25), calls=%async_computation.2 | async-start | bytes 4194304 | tf_op jit(solution)/shard_map/all_to_all | solution.py:221
  139.4 59.5 %all-gather.6.cloned.1.call-start = ((), (), s32[]{:S(2)}) async-start(), calls=%async_computation.5 | async-start | bytes 1310720 | tf_op jit(solution)/shard_map/all_gather | solution.py:195
  195.3 52.1 %all-to-all-start.1 = ((bf16[8,64,2048]{2,1,0:T(8,128)(2,1)}), bf16[8,64,2048]{2,1,0:T(8,128)(2,1)S(1)}, u32[]{:S(2)}, u32[]{:S(2)}) async-start(bf16[8,64,2048]{2,1,0:T(8,128)(2,1)} %convolution_convert_fusion), calls=%async_computation.3 | async-start | bytes 4194304 | tf_op jit(solution)/shard_map/all_to_all | solution.py:234
  198.9 54.8 %reduce-scatter.5.cloned.1.call-start = ((), (), s32[]{:S(2)}) async-start(), calls=%async_computation.6 | async-start | bytes 1310720 | tf_op jit(solution)/shard_map/reduce_scatter | solution.py:196
  200.7 3.3 %copy-start.18 = (f32[64,4]{0,1:T(4,128)S(1)}, f32[64,4]{0,1:T(4,128)}, u32[]{:S(2)}) copy-start(f32[64,4]{0,1:T(4,128)} %param.43) | copy-start | bytes 3076
Sparse Core Ops, SparseCore 0:
  34.8 49.5 all-gather.7
  105.0 23.2 reduce-scatter.2
  141.8 17.1 all-gather.5
  204.2 25.1 reduce-scatter.4
where the time goes:
time: 263 us; the launch traced here: 262 us
  waiting for transfers between devices  132 us (50%)
  other arithmetic  29.3 us (11%)
  matrix products  24.9 us (9%)
  local copies, waits for them, and re-layouts  22.8 us (9%)
  starting transfers between devices  21.3 us (8%)
  blocking collectives  18.2 us (7%)
  between operations  13.7 us (5%)
    all_to_all x1, waiting for transfers between devices, shards(): lax.all_to_all(outgoing, 'sp', split_axis=0, concat_axis=0, tiled=True)  47.3 us
    all_to_all x1, waiting for transfers between devices, shards(): lax.all_to_all(result.reshape(arrived.shape), 'sp', split_axis=0, concat_...  43.2 us
    reduce_scatter x1, waiting for transfers between devices, shards(): lax.psum_scatter(jnp.dot(heads_out, mixer_output_weight, preferred_elemen...  20.5 us
    all_gather x1, waiting for transfers between devices, entering(): lax.all_gather(part.astype(kind), axis)  20.4 us
    all_gather x1, blocking collectives, entering(): lax.all_gather(part.astype(kind), axis)  18.2 us
    ppermute x3, starting transfers between devices, shifted(): lax.ppermute(value, axis, [(source, source + steps) for source in range(f...  11.7 us
    select_n x8, other arithmetic, hop(): return jax.tree.map(lambda a, b: jnp.where(reached, a, b), new, before)  8.79 us
    all_to_all x1, starting transfers between devices, shards(): lax.all_to_all(outgoing, 'sp', split_axis=0, concat_axis=0, tiled=True)  5.53 us
  transfers between devices with their start and end apart: 9, of which 4 were waited for; matrix products, arithmetic and copies ran while one was open for 14% of the time, Pallas kernels for 0%

commit v1 on v0

v1 whole, which is shorter than its diff:
```python
import functools

import jax
import jax.numpy as jnp
from jax import lax
from jax.experimental import pallas as pl
from jax.experimental.pallas import tpu as pltpu
from jax.sharding import PartitionSpec as P

HEAD_DIM = 64
STATE = 128
CONV = 4
EPSILON = 1e-06
EXACT = lax.Precision.HIGHEST
F32 = jnp.float32
BF16 = jnp.bfloat16


def head_lanes(heads):
    lane_head = lax.broadcasted_iota(jnp.int32, (heads, heads * HEAD_DIM), 1) // HEAD_DIM
    return (lane_head == lax.broadcasted_iota(jnp.int32, lane_head.shape, 0)).astype(F32)


def expand(per_head, lanes):
    return jnp.dot(per_head, lanes, precision=EXACT, preferred_element_type=F32)


def silu(value):
    return value / (1.0 + jnp.exp(-value))


def local_kernel(
    v_ref, b_ref, c_ref, rim_ref, pre_ref, extra_ref, rates_ref, skip_ref, vk_ref, bk_ref, ck_ref,
    state_ref, y_ref, readout_ref, cum_ref, v_ext, b_ext, c_ext,
):
    length, heads = pre_ref.shape
    groups = b_ref.shape[1] // STATE
    per_group = heads // groups
    pad = rim_ref.shape[0]

    def conv(x_ref, first, k_ref, ext):
        width = x_ref.shape[1]
        ext[:pad] = rim_ref[:, first : first + width].astype(F32)
        ext[pad:] = x_ref[...].astype(F32)
        total = jnp.zeros((length, width), F32)
        for tap in range(CONV):
            start = pad - CONV + 1 + tap
            total += ext[start : start + length] * k_ref[tap : tap + 1].astype(F32)
        return silu(total)

    step = pre_ref[...]
    step = jnp.maximum(step, 0.0) + jnp.log1p(jnp.exp(-jnp.abs(step)))
    log_decay = -jnp.exp(rates_ref[...]) * step + extra_ref[...]
    row = lax.broadcasted_iota(jnp.int32, (length, length), 0)
    column = lax.broadcasted_iota(jnp.int32, (length, length), 1)
    causal = row >= column
    cum = jnp.dot(causal.astype(F32), log_decay, precision=EXACT, preferred_element_type=F32)
    cum_ref[...] = cum
    cum_rows = cum.T
    lanes = head_lanes(heads)
    b = conv(b_ref, v_ref.shape[1], bk_ref, b_ext).astype(BF16)
    v = conv(v_ref, 0, vk_ref, v_ext)
    last = cum[length - 1 : length]
    weighted = v * expand(step, lanes)
    ending = (weighted * expand(jnp.exp(last - cum), lanes)).astype(BF16)
    weighted = weighted.astype(BF16)
    whole = expand(jnp.broadcast_to(last, (8, heads)), lanes)
    coarse = whole.astype(BF16)
    state_ref[STATE : STATE + 8] = coarse
    state_ref[STATE + 8 :] = (whole - coarse.astype(F32)).astype(BF16)
    for g in range(groups):
        span = slice(g * per_group * HEAD_DIM, (g + 1) * per_group * HEAD_DIM)
        state_ref[:STATE, span] = lax.dot_general(
            b[:, g * STATE : (g + 1) * STATE], ending[:, span], (((0,), (0,)), ((), ())),
            preferred_element_type=F32,
        ).astype(BF16)
    c = conv(c_ref, v_ref.shape[1] + b_ref.shape[1], ck_ref, c_ext).astype(BF16)
    readout_ref[...] = c
    direct = v * skip_ref[...]
    for g in range(groups):
        cols = slice(g * STATE, (g + 1) * STATE)
        scores = lax.dot_general(
            c[:, cols], b[:, cols], (((1,), (1,)), ((), ())), preferred_element_type=F32
        )
        for h in range(g * per_group, (g + 1) * per_group):
            span = slice(h * HEAD_DIM, (h + 1) * HEAD_DIM)
            logs = jnp.where(causal, cum[:, h : h + 1] - cum_rows[h : h + 1], -jnp.inf)
            mixed = (scores * jnp.exp(logs)).astype(BF16)
            y_ref[:, span] = direct[:, span] + jnp.dot(
                mixed, weighted[:, span], preferred_element_type=F32
            )


def joined_kernel(
    axis, states_ref, y_ref, readout_ref, cum_ref, gate_ref, gain_ref, out_w_ref, out_ref, heads_ref
):
    me = lax.axis_index(axis)
    count = states_ref.shape[0]
    length, heads = cum_ref.shape
    groups = readout_ref.shape[1] // STATE
    per_group = heads // groups
    width = heads * HEAD_DIM

    def hop(turn, carry):
        total, run = carry
        k = count - 1 - turn
        earlier = k < me
        block = states_ref[k].astype(F32)
        factor = jnp.where(earlier, jnp.exp(run), 0.0)
        total = total + factor * block[:STATE]
        span = block[STATE : STATE + 1] + block[STATE + 8 : STATE + 9]
        return total, run + jnp.where(earlier, span, 0.0)

    start = (jnp.zeros((STATE, width), F32), jnp.zeros((1, width), F32))
    incoming = lax.fori_loop(0, count, hop, start)[0].astype(BF16)
    lanes = head_lanes(heads)
    decayed = expand(jnp.exp(cum_ref[...]), lanes)
    parts = [
        jnp.dot(
            readout_ref[:, g * STATE : (g + 1) * STATE],
            incoming[:, g * per_group * HEAD_DIM : (g + 1) * per_group * HEAD_DIM],
            preferred_element_type=F32,
        )
        for g in range(groups)
    ]
    mixed = y_ref[...] + jnp.concatenate(parts, axis=1) * decayed
    mixed = mixed * silu(gate_ref[...].astype(F32))
    squares = lax.dot_general(
        mixed * mixed, lanes, (((1,), (1,)), ((), ())), precision=EXACT, preferred_element_type=F32
    )
    scale = expand(lax.rsqrt(squares / HEAD_DIM + EPSILON), lanes)
    heads_ref[...] = (mixed * scale * gain_ref[...]).astype(BF16)
    tile = 512
    for first in range(0, out_w_ref.shape[1], tile):
        out_ref[:, first : first + tile] = jnp.dot(
            heads_ref[...], out_w_ref[:, first : first + tile], preferred_element_type=F32
        ).astype(BF16)


VMEM = pl.BlockSpec(memory_space=pltpu.VMEM)


def mixer(
    output_gate, value, state, readout, pre, extra, vk, bk, ck, rates, skip, gain, out_weight
):
    length, heads = pre.shape
    width = value.shape[1]
    count = lax.axis_size("sp")
    tails = jnp.concatenate([x[length - 8 :] for x in (value, state, readout)], axis=1)
    rim = lax.ppermute(tails, "sp", [(k, k + 1) for k in range(count - 1)])
    shape = jax.ShapeDtypeStruct
    states, y, c, cum = pl.pallas_call(
        local_kernel,
        out_shape=(
            shape((STATE + 16, width), BF16),
            shape((length, width), F32),
            shape(readout.shape, BF16),
            shape((length, heads), F32),
        ),
        in_specs=[VMEM] * 11,
        out_specs=(VMEM,) * 4,
        scratch_shapes=[
            pltpu.VMEM((length + 8, width), F32),
            pltpu.VMEM((length + 8, state.shape[1]), F32),
            pltpu.VMEM((length + 8, readout.shape[1]), F32),
        ],
        compiler_params=pltpu.CompilerParams(vmem_limit_bytes=48 << 20),
        cost_estimate=pl.CostEstimate(flops=10**9, bytes_accessed=4 * 10**6, transcendentals=10**6),
    )(
        value, state, readout, rim, pre, extra, rates[None],
        jnp.repeat(skip, HEAD_DIM)[None], vk, bk, ck,
    )
    gathered = lax.all_gather(states, "sp")
    return pl.pallas_call(
        functools.partial(joined_kernel, "sp"),
        out_shape=shape((length, out_weight.shape[1]), BF16),
        in_specs=[VMEM] * 7,
        out_specs=VMEM,
        scratch_shapes=[pltpu.VMEM((length, width), BF16)],
        compiler_params=pltpu.CompilerParams(vmem_limit_bytes=56 << 20),
        cost_estimate=pl.CostEstimate(flops=10**9, bytes_accessed=9 * 10**6, transcendentals=10**6),
    )(gathered, y, c, cum, output_gate, gain[None], out_weight)


def shared_slices(gate, up, down):
    count, parts = lax.axis_size("sp"), lax.axis_size("tp")
    held = gate.shape[1]
    piece = held * parts // count
    s, t = lax.axis_index("sp"), lax.axis_index("tp")
    first = (s * piece) % held
    mine = jnp.concatenate(
        [lax.dynamic_slice_in_dim(w, first, piece, axis=1) for w in (gate, up, down)], axis=1
    )
    owner = [(k * piece) // held for k in range(count)]
    total = jnp.where(t == (s * piece) // held, mine, jnp.zeros_like(mine))
    for d in range(1, parts):
        pairs = [(k * parts + o, k * parts + (o + d) % parts) for k, o in enumerate(owner)]
        total = total + lax.ppermute(mine, ("sp", "tp"), pairs)
    return total[:, :piece], total[:, piece : 2 * piece], total[:, 2 * piece :]


def shards(
    residual,
    output_gate_projected,
    value_projected_input,
    state_projected_input,
    readout_projected_input,
    step_preactivation,
    position_decay_extra,
    value_conv_kernel,
    state_conv_kernel,
    readout_conv_kernel,
    head_log_decay_rates,
    head_direct_weight,
    head_norm_gain,
    mixer_output_weight,
    expert_norm_gain,
    routed_expert_index,
    routed_expert_weight,
    routed_gate_weight,
    routed_up_weight,
    routed_down_weight,
    common_gate_weight,
    common_up_weight,
    common_down_weight,
):
    shared_gate, shared_up, shared_down = shared_slices(
        common_gate_weight, common_up_weight, common_down_weight
    )
    partial_mix = mixer(
        output_gate_projected, value_projected_input, state_projected_input,
        readout_projected_input, step_preactivation, position_decay_extra, value_conv_kernel,
        state_conv_kernel, readout_conv_kernel, head_log_decay_rates, head_direct_weight,
        head_norm_gain, mixer_output_weight,
    )
    count = lax.axis_size("sp")
    local_experts = routed_gate_weight.shape[0]
    experts_all = local_experts * count
    row_count, features = residual.shape
    chosen = jnp.arange(experts_all, dtype=jnp.int32) == routed_expert_index[:, :, None]
    combine = jnp.sum(jnp.where(chosen, routed_expert_weight[:, :, None], 0.0), axis=1)
    combine_high = combine.astype(BF16)
    combine_low = (combine - combine_high.astype(F32)).astype(BF16)
    extra_lanes = -(-2 * experts_all // 128) * 128 - 2 * experts_all

    mix_sum = lax.psum_scatter(partial_mix, "tp", scatter_dimension=0, tiled=True).astype(F32)
    stream = (residual.astype(F32) + mix_sum).astype(BF16)
    stream_wide = stream.astype(F32)
    normed_rows = (
        stream_wide
        * lax.rsqrt(jnp.mean(stream_wide * stream_wide, axis=-1, keepdims=True) + EPSILON)
        * expert_norm_gain
    ).astype(BF16)
    packed = jnp.concatenate(
        [normed_rows, combine_high, combine_low, jnp.zeros((row_count, extra_lanes), BF16)], axis=1
    )
    gathered = lax.all_gather(packed, "sp", axis=0, tiled=True)
    rows = gathered[:, :features]
    marks = gathered[:, features:].astype(F32)
    weights = marks[:, :experts_all] + marks[:, experts_all : 2 * experts_all]
    first = lax.axis_index("sp") * local_experts
    dot = functools.partial(jnp.dot, preferred_element_type=F32)
    hidden = (jax.nn.silu(dot(rows, shared_gate)) * dot(rows, shared_up)).astype(BF16)
    result = lax.dot_general(
        hidden, shared_down, (((1,), (1,)), ((), ())), preferred_element_type=F32
    )
    for e in range(local_experts):
        weight = lax.dynamic_slice_in_dim(weights, first + e, 1, axis=1)
        hidden = (
            jax.nn.silu(dot(rows, routed_gate_weight[e])) * dot(rows, routed_up_weight[e])
        ).astype(BF16)
        result = result + weight * dot(hidden, routed_down_weight[e])
    added = lax.psum_scatter(result.astype(BF16), "sp", scatter_dimension=0, tiled=True)
    return (stream_wide + added.astype(F32)).astype(BF16)


def solution(mesh):
    placed = (
        P(("sp", "tp"), None),
        P("sp", "tp"),
        P("sp", "tp"),
        P("sp", "tp"),
        P("sp", "tp"),
        P("sp", "tp"),
        P("sp", "tp"),
        P(None, "tp"),
        P(None, "tp"),
        P(None, "tp"),
        P("tp"),
        P("tp"),
        P("tp"),
        P("tp", None),
        P(),
        P(("sp", "tp"), None),
        P(("sp", "tp"), None),
        P("sp", None, None),
        P("sp", None, None),
        P("sp", None, None),
        P(None, "tp"),
        P(None, "tp"),
        P(None, "tp"),
    )
    return jax.shard_map(
        shards, mesh=mesh, in_specs=placed, out_specs=P(("sp", "tp"), None), check_vma=False
    )
```

time: 263 us -> 264 us (level)
  waiting for transfers between devices: 132 us -> 181 us
  other arithmetic: 29.3 us -> 8.3 us
  blocking collectives: 18.2 us -> 0 us
  Pallas kernels: 0 us -> 16.1 us
  matrix products: 24.9 us -> 15.6 us
  starting transfers between devices: 21.3 us -> 12.5 us
  local copies, waits for them, and re-layouts: 22.8 us -> 16.3 us
    all_to_all x2 -> x0, waiting for transfers between devices: 90.5 us -> none  [the longest x1 47.3 us: shards(): lax.all_to_all(outgoing, 'sp', split_axis=0, concat_axis=0, tiled=True)]
    reduce_scatter x2, waiting for transfers between devices: 20.5 us -> 90.2 us  [the longest x1 67.1 us: shards(): lax.psum_scatter(result.astype(BF16), 'sp', scatter_dimension=0, tiled=True)]
    all_gather x2, waiting for transfers between devices: 20.4 us -> 77.9 us  [the longest x1 53.1 us: mixer(): gathered = lax.all_gather(states, 'sp')]
    all_gather x1 -> x0, blocking collectives: 18.2 us -> none  [entering(): lax.all_gather(part.astype(kind), axis)]
    pallas_call x0 -> x2, Pallas kernels: none -> 16.1 us  [the longest x1 11.5 us: mixer(): pl.pallas_call(functools.partial(joined_kernel, 'sp'), out_shape=shape((l...]
    ppermute x3 -> x4, waiting for transfers between devices: 0.01 us -> 12.7 us  [the longest x3 12.7 us: shared_slices(): total = total + lax.ppermute(mine, ('sp', 'tp'), pairs)]
    select_n x12 -> x0, other arithmetic: 9.61 us -> none  [the longest x8 8.79 us: hop(): return jax.tree.map(lambda a, b: jnp.where(reached, a, b), new, before)]
    dot_general x9 -> x4, matrix products: 24.9 us -> 15.6 us  [the longest x1 5.6 us: shards(): result = result + weight * dot(hidden, routed_down_weight[e])]
  transfers between devices with their start and end apart: 9 -> 8, of which waited for: 4 -> 6; matrix products, arithmetic and copies ran while one was open for 14% -> 3% of each run, Pallas kernels for 0% -> 0%
where the time goes in v1:
time: 264 us; the launch traced here: 263 us
  waiting for transfers between devices  181 us (69%)
  local copies, waits for them, and re-layouts  16.3 us (6%)
  Pallas kernels  16.1 us (6%)
  matrix products  15.6 us (6%)
  between operations  13.3 us (5%)
  starting transfers between devices  12.5 us (5%)
  other arithmetic  8.3 us (3%)
    reduce_scatter x1, waiting for transfers between devices, shards(): lax.psum_scatter(result.astype(BF16), 'sp', scatter_dimension=0, tiled=True)  67.1 us
    all_gather x1, waiting for transfers between devices, mixer(): gathered = lax.all_gather(states, 'sp')  53.1 us
    all_gather x1, waiting for transfers between devices, shards(): gathered = lax.all_gather(packed, 'sp', axis=0, tiled=True)  24.8 us
    reduce_scatter x1, waiting for transfers between devices, shards(): lax.psum_scatter(partial_mix, 'tp', scatter_dimension=0, tiled=True)  23.1 us
    ppermute x3, waiting for transfers between devices, shared_slices(): total = total + lax.ppermute(mine, ('sp', 'tp'), pairs)  12.7 us
    pallas_call x1, Pallas kernels, mixer(): pl.pallas_call(functools.partial(joined_kernel, 'sp'), out_shape=shape((l...  11.5 us
    unnamed x43, local copies, waits for them, and re-layouts  10.2 us
    ppermute x3, starting transfers between devices, shared_slices(): total = total + lax.ppermute(mine, ('sp', 'tp'), pairs)  7.52 us
  transfers between devices with their start and end apart: 8, of which 6 were waited for; matrix products, arithmetic and copies ran while one was open for 3% of the time, Pallas kernels for 0%

profile of v1, /device:TPU:0, one launch (start us, length us, event | category | flops | bytes accessed | tf_op | source)
XLA Modules:
  0.0 262.9 jit_solution(7962982606805318992)
XLA Ops:
  6.5 0.0 copy-start
  6.5 0.0 all-gather.6.cloned.1.call-start
  6.5 0.8 slice.31
  7.3 0.7 slice.32
  8.0 0.7 slice.30
  8.8 4.9 %collective-permute-start = (bf16[8,2048]{1,0:T(8,128)(2,1)S(1)}, bf16[8,2048]{1,0:T(8,128)(2,1)S(1)}, u32[]{:S(2)}, u32[]{:S(2)}) collective-permute-start(bf16[8,2048]{1,0:T(8,128)(2,1)S(1)} %pad_maximum_fusion.1), channel_id=1, source_target_pairs={{0,4},{4,8},{8,12},{12,16},{16,20},{20,24},{24,28},{1,5},{5,9},{9,... | collective-permute-start | bytes 98312 | tf_op jit(solution)/shard_map/ppermute | solution.py:150
  13.6 0.7 broadcast_in_dim.33
  14.4 0.1 broadcast_in_dim_reshape.3.skip_ref
  14.5 0.8 copy.46.pre_ref
  15.3 0.8 copy.47.extra_ref
  16.1 0.0 collective-permute-done.rim_ref
  16.1 0.0 copy-start.4
  16.1 1.0 copy-done.4
  17.1 0.9 copy-done.5
  18.1 0.9 copy-done.6
  19.0 0.7 copy-done.7
  19.7 0.7 copy-done.8
  20.4 0.7 copy-done.9
  21.1 0.7 copy-done.10
  21.8 4.6 %shard_map.217 = (bf16[144,1024]{1,0:T(8,128)(2,1)}, f32[256,1024]{1,0:T(8,128)S(1)}, bf16[256,512]{1,0:T(8,128)(2,1)S(1)}, f32[256,16]{1,0:T(8,128)S(1)}) custom-call(bf16[256,1024]{1,0:T(8,128)(2,1)S(1)} %copy-done.4, bf16[256,512]{1,0:T(8,128)(2,1)S(1)} %copy-done.5, bf16[256,512]{1,0:T(8,128)(2,1)S(1)} %copy-done.6, ...), custom_call_target="tpu_custom_call" | custom-call | flops 1000000000 | bytes 4000000 | tf_op jit(solution)/shard_map/pallas_call | solution.py:152
  26.4 1.0 copy-done.1
  27.4 0.7 copy-done.2
  28.1 0.6 copy-done.3
  28.7 0.0 all-gather.6.cloned.1.call-update
  28.7 0.0 reduce-scatter.3.cloned.1.call-start
  28.8 53.1 %all-gather.6.cloned.1.call-done = bf16[1152,1024]{1,0:T(8,128)(2,1)} async-done(((bf16[144,1024]{1,0:T(8,128)(2,1)}), bf16[1152,1024]{1,0:T(8,128)(2,1)}) %all-gather.6.cloned.1.call-update) | async-done | bytes 2359312 | tf_op jit(solution)/shard_map/all_gather | solution.py:173
  81.9 11.5 %shard_map.218 = bf16[256,2048]{1,0:T(8,128)(2,1)} custom-call(bf16[8,144,1024]{2,1,0:T(8,128)(2,1)} %bitcast.14, f32[256,1024]{1,0:T(8,128)} %copy-done.1, bf16[256,512]{1,0:T(8,128)(2,1)} %copy-done.2, f32[256,16]{1,0:T(8,128)} %copy-done.3, bf16[256,1024]{1,0:T(8,128)(2,1)} %gate_ref.1, f32[1,1024]{1,0:T(1,128)} %bitcast.15, bf16[1024,2048]{1,0:T(8,128)(2,1)} %out_w_ref.1), custom_call_target="tpu_custom_call" | custom-call | flops 1000000000 | bytes 9000000 | tf_op jit(solution)/shard_map/pallas_call | solution.py:174
  93.4 0.0 reduce-scatter.3.cloned.1.call-update
  93.4 0.0 all-gather.4.cloned.1.call-start
  93.5 0.1 copy.48
  93.6 0.1 copy.50
  93.7 0.1 copy.49
  93.8 23.1 %reduce-scatter.3.cloned.1.call-done = bf16[64,2048]{1,0:T(8,128)(2,1)} async-done(((bf16[256,2048]{1,0:T(8,128)(2,1)}), bf16[64,2048]{1,0:T(8,128)(2,1)}) %reduce-scatter.3.cloned.1.call-update) | async-done | bytes 262160 | tf_op jit(solution)/shard_map/reduce_scatter | solution.py:246
  116.9 1.1 fusion.21
  118.0 1.1 fusion.23
  119.1 0.8 concatenate.10
  119.9 0.0 all-gather.4.cloned.1.call-update
  119.9 0.0 reduce-scatter.5.cloned.1.call-start
  120.0 0.2 constant_dynamic-slice_fusion.2
  120.2 0.2 copy.54
  120.4 1.6 constant_dynamic-slice_fusion
  122.0 0.2 copy.56
  122.2 0.2 copy.55
  122.4 0.1 pad_maximum_fusion
  122.5 3.2 %collective-permute-start.2 = (bf16[2048,192]{0,1:T(8,128)(2,1)S(1)}, bf16[2048,192]{0,1:T(8,128)(2,1)}, u32[]{:S(2)}, u32[]{:S(2)}) collective-permute-start(bf16[2048,192]{0,1:T(8,128)(2,1)S(1)} %pad_maximum_fusion), channel_id=1, source_target_pairs={{0,2},{4,6},{9,11},{13,15},{18,16},{22,20},{27,25},{31,29}} | collective-permute-start | bytes 2359304 | tf_op jit(solution)/shard_map/ppermute | solution.py:198
  125.7 2.2 collective-permute-start.1
  127.8 2.2 collective-permute-start.3
  130.0 4.2 %collective-permute-done.2 = bf16[2048,192]{0,1:T(8,128)(2,1)} collective-permute-done((bf16[2048,192]{0,1:T(8,128)(2,1)S(1)}, bf16[2048,192]{0,1:T(8,128)(2,1)}, u32[]{:S(2)}, u32[]{:S(2)}) %collective-permute-start.2) | collective-permute-done | bytes 786464 | tf_op jit(solution)/shard_map/ppermute | solution.py:198
  134.2 0.0 collective-permute-done.1
  134.2 8.4 %collective-permute-done.3 = bf16[2048,192]{0,1:T(8,128)(2,1)} collective-permute-done((bf16[2048,192]{0,1:T(8,128)(2,1)S(1)}, bf16[2048,192]{0,1:T(8,128)(2,1)}, u32[]{:S(2)}, u32[]{:S(2)}) %collective-permute-start.3) | collective-permute-done | bytes 786464 | tf_op jit(solution)/shard_map/ppermute | solution.py:198
  142.7 3.0 %add_add_fusion = bf16[2048,192]{0,1:T(8,128)(2,1)} fusion(bf16[2048,192]{0,1:T(8,128)(2,1)} %collective-permute-done.3, bf16[2048,192]{0,1:T(8,128)(2,1)} %collective-permute-done.2, bf16[2048,192]{0,1:T(8,128)(2,1)} %collective-permute-done.1, pred[]{:T(512)S(6)} %eq.21, bf16[2048,64]{0,1:T(8,128)(2,1)S(1)} %copy.56, bf16[2048,64]{0,1:T(8,128)(2,1)S(1)} %copy.55, ...), kind=kLoop, calls=%fused_computation.16 | loop fusion | flops 5898240 | bytes 3932161 | tf_op jit(solution)/shard_map/add | solution.py:198
  145.7 24.8 %all-gather.4.cloned.1.call-done = bf16[512,2176]{1,0:T(8,128)(2,1)} async-done(((bf16[64,2176]{1,0:T(8,128)(2,1)}), bf16[512,2176]{1,0:T(8,128)(2,1)}) %all-gather.4.cloned.1.call-update) | async-done | bytes 2228240 | tf_op jit(solution)/shard_map/all_gather | solution.py:257
  170.5 0.9 slice_convert_fusion
  171.4 0.1 fusion.46
  171.6 0.0 copy-start.18
  171.6 0.3 fusion.30
  171.9 3.2 %fusion.4 = f32[512,64]{0,1:T(8,128)} fusion(bf16[512,2176]{1,0:T(8,128)(2,1)} %all-gather.4.cloned.1.call-done, bf16[2048,192]{0,1:T(8,128)(2,1)} %add_add_fusion), kind=kOutput, calls=%fused_computation.5 | convolution fusion | flops 134217728 | bytes 2490368 | tf_op jit(solution)/shard_map/dot_general | solution.py:263
  175.1 1.5 fusion.2
  176.6 0.0 copy-done
  176.6 5.6 %fusion.15 = f32[512,2048]{1,0:T(8,128)} fusion(bf16[512,2176]{1,0:T(8,128)(2,1)S(1)} %copy-done.11, bf16[1,256,2048]{2,1,0:T(8,128)(2,1)S(1)} %copy-done, bf16[1,2048,256]{2,1,0:T(8,128)(2,1)} %param.41, f32[512,256]{1,0:T(8,128)} %fusion.2), kind=kOutput, calls=%fused_computation.11 | convolution fusion | flops 1074528256 | bytes 8912896 | tf_op jit(solution)/shard_map/dot_general | solution.py:272
  182.2 5.3 %add_convert_fusion = bf16[512,2048]{1,0:T(8,128)(2,1)} fusion(f32[512,2048]{1,0:T(8,128)} %fusion.15, f32[512]{0:T(512)S(1)} %fusion.30, bf16[2048,192]{0,1:T(8,128)(2,1)} %add_add_fusion, f32[512,64]{0,1:T(8,128)} %fusion.4, bf16[512,2176]{1,0:T(8,128)(2,1)S(1)} %copy-done.11), kind=kOutput, calls=%fused_computation | convolution fusion | flops 271777792 | bytes 9046016 | tf_op jit(solution)/shard_map/dot_general | solution.py:264
  187.5 0.0 reduce-scatter.5.cloned.1.call-update
  187.5 67.1 %reduce-scatter.5.cloned.1.call-done = bf16[64,2048]{1,0:T(8,128)(2,1)} async-done(((bf16[512,2048]{1,0:T(8,128)(2,1)}), bf16[64,2048]{1,0:T(8,128)(2,1)}) %reduce-scatter.5.cloned.1.call-update) | async-done | bytes 262160 | tf_op jit(solution)/shard_map/reduce_scatter | solution.py:273
  254.6 1.7 fusion.24
  (30 shorter events, 0.1 us)
Async XLA Ops:
  6.5 170.1 %copy-start = (bf16[1,256,2048]{2,1,0:T(8,128)(2,1)S(1)}, bf16[1,256,2048]{2,1,0:T(8,128)(2,1)}, u32[]{:S(2)}) copy-start(bf16[1,256,2048]{2,1,0:T(8,128)(2,1)} %param.42) | copy-start | bytes 3145732
  6.5 75.3 %all-gather.6.cloned.1.call-start = ((), (), s32[]{:S(2)}) async-start(), calls=%async_computation.5 | async-start | bytes 2654208 | tf_op jit(solution)/shard_map/all_gather | solution.py:173
  8.8 7.3 %collective-permute-start = (bf16[8,2048]{1,0:T(8,128)(2,1)S(1)}, bf16[8,2048]{1,0:T(8,128)(2,1)S(1)}, u32[]{:S(2)}, u32[]{:S(2)}) collective-permute-start(bf16[8,2048]{1,0:T(8,128)(2,1)S(1)} %pad_maximum_fusion.1), channel_id=1, source_target_pairs={{0,4},{4,8},{8,12},{12,16},{16,20},{20,24},{24,28},{1,5},{5,9},{9,... | collective-permute-start | bytes 98312 | tf_op jit(solution)/shard_map/ppermute | solution.py:150
  16.1 1.0 copy-start.4
  17.1 0.9 copy-start.5
  18.1 0.9 copy-start.6
  19.0 0.7 copy-start.7
  19.7 0.7 copy-start.8
  20.4 0.7 copy-start.9
  21.1 0.7 copy-start.10
  26.4 1.0 copy-start.1
  27.4 0.7 copy-start.2
  28.1 0.7 copy-start.3
  28.7 88.1 %reduce-scatter.3.cloned.1.call-start = ((), (), s32[]{:S(2)}) async-start(), calls=%async_computation.2 | async-start | bytes 1310720 | tf_op jit(solution)/shard_map/reduce_scatter | solution.py:246
  81.9 11.6 %copy-start.16 = (f32[64,4]{0,1:T(4,128)S(1)}, f32[64,4]{0,1:T(4,128)}, u32[]{:S(2)}) copy-start(f32[64,4]{0,1:T(4,128)} %param.39) | copy-start | bytes 3076
  81.9 11.6 %copy-start.17 = (s32[64,4]{0,1:T(4,128)S(1)}, s32[64,4]{0,1:T(4,128)}, u32[]{:S(2)}) copy-start(s32[64,4]{0,1:T(4,128)} %param.38) | copy-start | bytes 3076
  81.9 35.0 %copy-start.12 = (bf16[64,2048]{1,0:T(8,128)(2,1)S(1)}, bf16[64,2048]{1,0:T(8,128)(2,1)}, u32[]{:S(2)}) copy-start(bf16[64,2048]{1,0:T(8,128)(2,1)} %param.23) | copy-start | bytes 786436
  81.9 36.1 %copy-start.15 = (f32[2048]{0:T(1024)S(1)}, f32[2048]{0:T(1024)}, u32[]{:S(2)}) copy-start(f32[2048]{0:T(1024)} %param.37) | copy-start | bytes 24580
  93.4 26.6 %copy-start.14 = (bf16[2048,128]{1,0:T(8,128)(2,1)S(1)}, bf16[2048,128]{1,0:T(8,128)(2,1)}, u32[]{:S(2)}) copy-start(bf16[2048,128]{1,0:T(8,128)(2,1)} %param.43) | copy-start | bytes 1572868
  93.4 77.1 %all-gather.4.cloned.1.call-start = ((), (), s32[]{:S(2)}) async-start(), calls=%async_computation.3 | async-start | bytes 2506752 | tf_op jit(solution)/shard_map/all_gather | solution.py:257
  119.9 134.6 %reduce-scatter.5.cloned.1.call-start = ((), (), s32[]{:S(2)}) async-start(), calls=%async_computation.4 | async-start | bytes 2359296 | tf_op jit(solution)/shard_map/reduce_scatter | solution.py:273
  122.5 11.8 %collective-permute-start.2 = (bf16[2048,192]{0,1:T(8,128)(2,1)S(1)}, bf16[2048,192]{0,1:T(8,128)(2,1)}, u32[]{:S(2)}, u32[]{:S(2)}) collective-permute-start(bf16[2048,192]{0,1:T(8,128)(2,1)S(1)} %pad_maximum_fusion), channel_id=1, source_target_pairs={{0,2},{4,6},{9,11},{13,15},{18,16},{22,20},{27,25},{31,29}} | collective-permute-start | bytes 2359304 | tf_op jit(solution)/shard_map/ppermute | solution.py:198
  125.7 8.6 %collective-permute-start.1 = (bf16[2048,192]{0,1:T(8,128)(2,1)S(1)}, bf16[2048,192]{0,1:T(8,128)(2,1)}, u32[]{:S(2)}, u32[]{:S(2)}) collective-permute-start(bf16[2048,192]{0,1:T(8,128)(2,1)S(1)} %pad_maximum_fusion), channel_id=1, source_target_pairs={{0,1},{4,5},{9,10},{13,14},{18,19},{22,23},{27,24},{31,28}} | collective-permute-start | bytes 2359304 | tf_op jit(solution)/shard_map/ppermute | solution.py:198
  127.8 14.8 %collective-permute-start.3 = (bf16[2048,192]{0,1:T(8,128)(2,1)S(1)}, bf16[2048,192]{0,1:T(8,128)(2,1)}, u32[]{:S(2)}, u32[]{:S(2)}) collective-permute-start(bf16[2048,192]{0,1:T(8,128)(2,1)S(1)} %pad_maximum_fusion), channel_id=1, source_target_pairs={{0,3},{4,7},{9,8},{13,12},{18,17},{22,21},{27,26},{31,30}} | collective-permute-start | bytes 2359304 | tf_op jit(solution)/shard_map/ppermute | solution.py:198
  171.6 3.5 %copy-start.11 = (bf16[512,2176]{1,0:T(8,128)(2,1)S(1)}, bf16[512,2176]{1,0:T(8,128)(2,1)}, u32[]{:S(2)}) copy-start(bf16[512,2176]{1,0:T(8,128)(2,1)} %all-gather.4.cloned.1.call-done) | copy-start | bytes 6684676
  171.6 3.5 %copy-start.18 = (bf16[1,2048,256]{2,1,0:T(8,128)(2,1)S(1)}, bf16[1,2048,256]{2,1,0:T(8,128)(2,1)}, u32[]{:S(2)}) copy-start(bf16[1,2048,256]{2,1,0:T(8,128)(2,1)} %param.40) | copy-start | bytes 3145732
  187.5 67.1 %copy-start.13 = (bf16[64,2048]{1,0:T(8,128)(2,1)S(1)}, bf16[64,2048]{1,0:T(8,128)(2,1)}, u32[]{:S(2)}) copy-start(bf16[64,2048]{1,0:T(8,128)(2,1)} %reduce-scatter.3.cloned.1.call-done) | copy-start | bytes 786436
Sparse Core Ops, SparseCore 0:
  28.9 52.9 all-gather.5
  93.5 23.2 reduce-scatter.2
  120.1 50.3 all-gather.3
  187.6 66.9 reduce-scatter.4

commit v2 on v1

--- a/solution.py
+++ b/solution.py
@@ -140,8 +140,312 @@
 VMEM = pl.BlockSpec(memory_space=pltpu.VMEM)
 
 
+MESH = pl.DeviceIdType.MESH
+CUTS = 2
+
+
+def greet(peers):
+    barrier = pltpu.get_barrier_semaphore()
+    for here, peer, axis in peers:
+        @pl.when(here)
+        def _():
+            pl.semaphore_signal(barrier, inc=1, device_id={axis: peer}, device_id_type=MESH)
+    pl.semaphore_wait(barrier, sum(jnp.where(here, 1, 0) for here, _, _ in peers))
+
+
+def gather_kernel(spread, lines, *refs):
+    if spread is None:
+        x_ref, out_ref, sent, landed = refs
+    else:
+        x_ref, mine_ref, out_ref, slices_ref, sent, landed, spread_sent, spread_landed = refs
+    me = lax.axis_index("sp")
+    z, y = me // 2, me % 2
+    half = x_ref.shape[0] // CUTS
+    always = me >= 0
+    peers = [
+        (always, me + 1 - 2 * y, "sp"), (z > 0, me - 2, "sp"), (z < lines - 1, me + 2, "sp")
+    ]
+    if spread is not None:
+        piece, held, parts = spread
+        t = lax.axis_index("tp")
+        owner = (me * piece) // held
+        peers += [(always, (t + d) % parts, "tp") for d in range(1, parts)]
+    greet(peers)
+
+    def send(block, cut, way, peer, first):
+        rows = pl.ds(cut * half, half)
+        return pltpu.make_async_remote_copy(
+            src_ref=x_ref.at[rows] if first else out_ref.at[block, rows],
+            dst_ref=out_ref.at[block, rows],
+            send_sem=sent.at[way, block, cut],
+            recv_sem=landed.at[block, cut],
+            device_id={"sp": peer},
+            device_id_type=MESH,
+        )
+
+    for cut in range(CUTS):
+        for way, (here, peer, _) in enumerate(peers[:3]):
+            @pl.when(here)
+            def _():
+                send(me, cut, way, peer, True).start()
+    if spread is not None:
+        def share(d):
+            return pltpu.make_async_remote_copy(
+                src_ref=mine_ref, dst_ref=slices_ref, send_sem=spread_sent.at[d - 1],
+                recv_sem=spread_landed.at[0], device_id={"tp": (t + d) % parts},
+                device_id_type=MESH,
+            )
+
+        @pl.when(t == owner)
+        def _():
+            for d in range(1, parts):
+                share(d).start()
+            slices_ref[...] = mine_ref[...]
+
+    out_ref[me] = x_ref[...]
+    for turn in range(1, lines):
+        for cut in range(CUTS):
+            for step, onward in ((-1, 2), (1, 1)):
+                far = z + step * turn
+                block = far * 2 + y
+
+                @pl.when((far >= 0) & (far < lines))
+                def _():
+                    send(block, cut, 0, peers[0][1], False).wait_recv()
+                    send(block, cut, 0, peers[0][1], False).start()
+
+                    @pl.when(peers[onward][0])
+                    def _():
+                        send(block, cut, onward, peers[onward][1], False).start()
+
+    for line in range(lines):
+        for cut in range(CUTS):
+            send(line * 2 + 1 - y, cut, 0, peers[0][1], False).wait_recv()
+    for cut in range(CUTS):
+        for line in range(lines):
+            send(line * 2 + y, cut, 0, peers[0][1], False).wait_send()
+
+            @pl.when((line <= z) & peers[2][0])
+            def _():
+                send(line * 2 + y, cut, 2, peers[2][1], False).wait_send()
+
+            @pl.when((line >= z) & peers[1][0])
+            def _():
+                send(line * 2 + y, cut, 1, peers[1][1], False).wait_send()
+
+    if spread is not None:
+        @pl.when(t == owner)
+        def _():
+            for d in range(1, parts):
+                share(d).wait_send()
+
+        @pl.when(t != owner)
+        def _():
+            share(1).wait_recv()
+
+
+def gather_sp(x, number, mine=None, held=0):
+    count, parts = lax.axis_size("sp"), lax.axis_size("tp")
+    shape = jax.ShapeDtypeStruct
+    lands = [shape((count, *x.shape), x.dtype)]
+    sems = [pltpu.SemaphoreType.DMA((3, count, CUTS)), pltpu.SemaphoreType.DMA((count, CUTS))]
+    operands, spread = [x], None
+    if mine is not None:
+        spread = (mine.shape[1] // 3, held, parts)
+        operands.append(mine)
+        lands.append(shape(mine.shape, mine.dtype))
+        sems += [pltpu.SemaphoreType.DMA((parts - 1,)), pltpu.SemaphoreType.DMA((1,))]
+    return pl.pallas_call(
+        functools.partial(gather_kernel, spread, count // 2),
+        out_shape=tuple(lands),
+        in_specs=[VMEM] * len(operands),
+        out_specs=(VMEM,) * len(lands),
+        scratch_shapes=sems,
+        compiler_params=pltpu.CompilerParams(
+            collective_id=number, has_side_effects=True, vmem_limit_bytes=24 << 20
+        ),
+    )(*operands)
+
+
+def reduce_sp_kernel(lines, x_ref, out_ref, across, along, staged, sent, landed, z_sent, z_landed):
+    me = lax.axis_index("sp")
+    z, y = me // 2, me % 2
+    other = me + 1 - 2 * y
+    half = out_ref.shape[0] // CUTS
+    greet([(me >= 0, other, "sp"), (z > 0, me - 2, "sp"), (z < lines - 1, me + 2, "sp")])
+
+    def cross(line, cut):
+        rows = pl.ds(cut * half, half)
+        return pltpu.make_async_remote_copy(
+            src_ref=x_ref.at[line * 2 + 1 - y, rows], dst_ref=across.at[line, rows],
+            send_sem=sent.at[line, cut], recv_sem=landed.at[line, cut],
+            device_id={"sp": other}, device_id_type=MESH,
+        )
+
+    def forward(line, slot, cut, step):
+        rows = pl.ds(cut * half, half)
+        return pltpu.make_async_remote_copy(
+            src_ref=staged.at[line, rows], dst_ref=along.at[slot, rows],
+            send_sem=z_sent.at[line, cut], recv_sem=z_landed.at[slot, cut],
+            device_id={"sp": me + 2 * step}, device_id_type=MESH,
+        )
+
+    for turn in reversed(range(lines)):
+        for cut in range(CUTS):
+            for step in (-1, 1) if turn else (1,):
+                line = z + step * turn
+
+                @pl.when((line >= 0) & (line < lines))
+                def _():
+                    cross(line, cut).start()
+
+    def met(line, cut):
+        rows = pl.ds(cut * half, half)
+        cross(line, cut).wait_recv()
+        return x_ref[line * 2 + y, rows].astype(F32) + across[line, rows].astype(F32)
+
+    for turn in reversed(range(1, lines)):
+        for cut in range(CUTS):
+            rows = pl.ds(cut * half, half)
+            for step in (-1, 1):
+                line = z + step * turn
+                behind = z - step
+                inside = (line >= 0) & (line < lines)
+                fed = (behind >= 0) & (behind < lines)
+                slot = jnp.where((turn == 1) & (step < 0), lines, line)
+
+                @pl.when(inside & fed)
+                def _():
+                    value = met(line, cut)
+                    forward(line, line, cut, step).wait_recv()
+                    staged[line, rows] = (value + along[line, rows].astype(F32)).astype(BF16)
+
+                @pl.when(inside & jnp.logical_not(fed))
+                def _():
+                    staged[line, rows] = met(line, cut).astype(BF16)
+
+                @pl.when(inside)
+                def _():
+                    forward(line, slot, cut, step).start()
+
+    for cut in range(CUTS):
+        rows = pl.ds(cut * half, half)
+        staged[z, rows] = met(z, cut).astype(BF16)
+
+        @pl.when(z > 0)
+        def _():
+            forward(z, z, cut, 1).wait_recv()
+            staged[z, rows] = (staged[z, rows].astype(F32) + along[z, rows].astype(F32)).astype(BF16)
+
+        @pl.when(z < lines - 1)
+        def _():
+            forward(z, lines, cut, -1).wait_recv()
+            staged[z, rows] = (
+                staged[z, rows].astype(F32) + along[lines, rows].astype(F32)
+            ).astype(BF16)
+
+        out_ref[rows] = staged[z, rows]
+        for line in range(lines):
+            cross(line, cut).wait_send()
+
+            @pl.when(line != z)
+            def _():
+                forward(line, line, cut, 0).wait_send()
+
+
+def reduce_sp(x, number):
+    count = x.shape[0]
+    lines = count // 2
+    block = x.shape[1:]
+    return pl.pallas_call(
+        functools.partial(reduce_sp_kernel, lines),
+        out_shape=jax.ShapeDtypeStruct(block, x.dtype),
+        in_specs=[VMEM],
+        out_specs=VMEM,
+        scratch_shapes=[
+            pltpu.VMEM((lines, *block), x.dtype),
+            pltpu.VMEM((lines + 1, *block), x.dtype),
+            pltpu.VMEM((lines, *block), x.dtype),
+        ]
+        + [
+            pltpu.SemaphoreType.DMA((lines + extra, CUTS)) for extra in (0, 0, 0, 1)
+        ],
+        compiler_params=pltpu.CompilerParams(
+            collective_id=number, has_side_effects=True, vmem_limit_bytes=24 << 20
+        ),
+    )(x)
+
+
+def reduce_tp_kernel(x_ref, out_ref, near, staged, far, near_sent, near_landed, far_sent, far_landed):
+    t = lax.axis_index("tp")
+    a, b = t // 2, t % 2
+    partner, opposite = a * 2 + 1 - b, (1 - a) * 2 + b
+    always = t >= 0
+    greet([(always, partner, "tp"), (always, opposite, "tp")])
+
+    def swap(row):
+        return pltpu.make_async_remote_copy(
+            src_ref=x_ref.at[row * 2 + 1 - b], dst_ref=near.at[row],
+            send_sem=near_sent.at[row], recv_sem=near_landed.at[row],
+            device_id={"tp": partner}, device_id_type=MESH,
+        )
+
+    half = out_ref.shape[0] // CUTS
+
+    def pass_on(cut):
+        rows = pl.ds(cut * half, half)
+        return pltpu.make_async_remote_copy(
+            src_ref=staged.at[rows], dst_ref=far.at[rows],
+            send_sem=far_sent.at[cut], recv_sem=far_landed.at[cut],
+            device_id={"tp": opposite}, device_id_type=MESH,
+        )
+
+    swap(1 - a).start()
+    swap(a).start()
+    swap(1 - a).wait_recv()
+    for cut in range(CUTS):
+        rows = pl.ds(cut * half, half)
+        staged[rows] = (
+            x_ref[opposite, rows].astype(F32) + near[1 - a, rows].astype(F32)
+        ).astype(BF16)
+        pass_on(cut).start()
+    swap(a).wait_recv()
+    out_ref[...] = x_ref[t].astype(F32) + near[a].astype(F32)
+    for cut in range(CUTS):
+        rows = pl.ds(cut * half, half)
+        pass_on(cut).wait_recv()
+        out_ref[rows] += far[rows].astype(F32)
+        pass_on(cut).wait_send()
+    swap(0).wait_send()
+    swap(1).wait_send()
+
+
+def reduce_tp(x, number):
+    parts, block = x.shape[0], x.shape[1:]
+    return pl.pallas_call(
+        reduce_tp_kernel,
+        out_shape=jax.ShapeDtypeStruct(block, F32),
+        in_specs=[VMEM],
+        out_specs=VMEM,
+        scratch_shapes=[
+            pltpu.VMEM((parts // 2, *block), x.dtype),
+            pltpu.VMEM(block, x.dtype),
+            pltpu.VMEM(block, x.dtype),
+        ]
+        + [pltpu.SemaphoreType.DMA((2,))] * 2 + [pltpu.SemaphoreType.DMA((CUTS,))] * 2,
+        compiler_params=pltpu.CompilerParams(
+            collective_id=number, has_side_effects=True, vmem_limit_bytes=16 << 20
+        ),
+    )(x)
+
+
+def small_mesh():
+    return lax.axis_size("sp") in (4, 8) and lax.axis_size("tp") == 4
+
+
 def mixer(
-    output_gate, value, state, readout, pre, extra, vk, bk, ck, rates, skip, gain, out_weight
+    output_gate, value, state, readout, pre, extra, vk, bk, ck, rates, skip, gain, out_weight,
+    common,
 ):
     length, heads = pre.shape
     width = value.shape[1]
@@ -170,8 +474,12 @@
         value, state, readout, rim, pre, extra, rates[None],
         jnp.repeat(skip, HEAD_DIM)[None], vk, bk, ck,
     )
-    gathered = lax.all_gather(states, "sp")
-    return pl.pallas_call(
+    if small_mesh():
+        gathered, slices = gather_sp(states, 1, own_slices(*common), common[0].shape[1])
+    else:
+        gathered = lax.all_gather(states, "sp")
+        slices = permuted_slices(*common)
+    partial = pl.pallas_call(
         functools.partial(joined_kernel, "sp"),
         out_shape=shape((length, out_weight.shape[1]), BF16),
         in_specs=[VMEM] * 7,
@@ -180,23 +488,30 @@
         compiler_params=pltpu.CompilerParams(vmem_limit_bytes=56 << 20),
         cost_estimate=pl.CostEstimate(flops=10**9, bytes_accessed=9 * 10**6, transcendentals=10**6),
     )(gathered, y, c, cum, output_gate, gain[None], out_weight)
-
-
-def shared_slices(gate, up, down):
+    return partial, slices
+
+
+def own_slices(gate, up, down):
+    held = gate.shape[1]
+    piece = held * lax.axis_size("tp") // lax.axis_size("sp")
+    first = (lax.axis_index("sp") * piece) % held
+    return jnp.concatenate(
+        [lax.dynamic_slice_in_dim(w, first, piece, axis=1) for w in (gate, up, down)], axis=1
+    )
+
+
+def permuted_slices(gate, up, down):
     count, parts = lax.axis_size("sp"), lax.axis_size("tp")
     held = gate.shape[1]
-    piece = held * parts // count
-    s, t = lax.axis_index("sp"), lax.axis_index("tp")
-    first = (s * piece) % held
-    mine = jnp.concatenate(
-        [lax.dynamic_slice_in_dim(w, first, piece, axis=1) for w in (gate, up, down)], axis=1
-    )
+    mine = own_slices(gate, up, down)
+    piece = mine.shape[1] // 3
     owner = [(k * piece) // held for k in range(count)]
-    total = jnp.where(t == (s * piece) // held, mine, jnp.zeros_like(mine))
+    here = lax.axis_index("tp") == (lax.axis_index("sp") * piece) // held
+    total = jnp.where(here, mine, jnp.zeros_like(mine))
     for d in range(1, parts):
         pairs = [(k * parts + o, k * parts + (o + d) % parts) for k, o in enumerate(owner)]
         total = total + lax.ppermute(mine, ("sp", "tp"), pairs)
-    return total[:, :piece], total[:, piece : 2 * piece], total[:, 2 * piece :]
+    return total
 
 
 def shards(
@@ -224,14 +539,16 @@
     common_up_weight,
     common_down_weight,
 ):
-    shared_gate, shared_up, shared_down = shared_slices(
-        common_gate_weight, common_up_weight, common_down_weight
-    )
-    partial_mix = mixer(
+    partial_mix, slices = mixer(
         output_gate_projected, value_projected_input, state_projected_input,
         readout_projected_input, step_preactivation, position_decay_extra, value_conv_kernel,
         state_conv_kernel, readout_conv_kernel, head_log_decay_rates, head_direct_weight,
         head_norm_gain, mixer_output_weight,
+        (common_gate_weight, common_up_weight, common_down_weight),
+    )
+    piece = slices.shape[1] // 3
+    shared_gate, shared_up, shared_down = (
+        slices[:, k * piece : (k + 1) * piece] for k in range(3)
     )
     count = lax.axis_size("sp")
     local_experts = routed_gate_weight.shape[0]
@@ -243,7 +560,10 @@
     combine_low = (combine - combine_high.astype(F32)).astype(BF16)
     extra_lanes = -(-2 * experts_all // 128) * 128 - 2 * experts_all
 
-    mix_sum = lax.psum_scatter(partial_mix, "tp", scatter_dimension=0, tiled=True).astype(F32)
+    if small_mesh():
+        mix_sum = reduce_tp(partial_mix.reshape(-1, row_count, features), 2)
+    else:
+        mix_sum = lax.psum_scatter(partial_mix, "tp", scatter_dimension=0, tiled=True).astype(F32)
     stream = (residual.astype(F32) + mix_sum).astype(BF16)
     stream_wide = stream.astype(F32)
     normed_rows = (
@@ -254,7 +574,10 @@
     packed = jnp.concatenate(
         [normed_rows, combine_high, combine_low, jnp.zeros((row_count, extra_lanes), BF16)], axis=1
     )
-    gathered = lax.all_gather(packed, "sp", axis=0, tiled=True)
+    if small_mesh():
+        gathered = gather_sp(packed, 3)[0].reshape(-1, packed.shape[1])
+    else:
+        gathered = lax.all_gather(packed, "sp", axis=0, tiled=True)
     rows = gathered[:, :features]
     marks = gathered[:, features:].astype(F32)
     weights = marks[:, :experts_all] + marks[:, experts_all : 2 * experts_all]
@@ -270,7 +593,11 @@
             jax.nn.silu(dot(rows, routed_gate_weight[e])) * dot(rows, routed_up_weight[e])
         ).astype(BF16)
         result = result + weight * dot(hidden, routed_down_weight[e])
-    added = lax.psum_scatter(result.astype(BF16), "sp", scatter_dimension=0, tiled=True)
+    result = result.astype(BF16)
+    if small_mesh():
+        added = reduce_sp(result.reshape(count, row_count, features), 4)
+    else:
+        added = lax.psum_scatter(result, "sp", scatter_dimension=0, tiled=True)
     return (stream_wide + added.astype(F32)).astype(BF16)
 
 

time: 264 us -> 145 us (0.55)
  waiting for transfers between devices: 181 us -> 0.01 us
  Pallas kernels: 16.1 us -> 109 us
  between operations: 13.3 us -> 0.35 us
  starting transfers between devices: 12.5 us -> 4.89 us
  other arithmetic: 8.3 us -> 2.96 us
    pallas_call x0 -> x4, Pallas kernels: none -> 92.5 us  [the longest x2 57.5 us: gather_sp(): pl.pallas_call(functools.partial(gather_kernel, spread, count // 2), out_...]
    reduce_scatter x2 -> x0, waiting for transfers between devices: 90.2 us -> none  [the longest x1 67.1 us: shards(): lax.psum_scatter(result.astype(BF16), 'sp', scatter_dimension=0, tiled=True)]
    all_gather x2 -> x0, waiting for transfers between devices: 77.9 us -> none  [the longest x1 53.1 us: mixer(): gathered = lax.all_gather(states, 'sp')]
    ppermute x3 -> x0, waiting for transfers between devices: 12.7 us -> none  [shared_slices(): total = total + lax.ppermute(mine, ('sp', 'tp'), pairs)]
    ppermute x3 -> x0, starting transfers between devices: 7.52 us -> none  [shared_slices(): total = total + lax.ppermute(mine, ('sp', 'tp'), pairs)]
    add x1, other arithmetic: 3.01 us -> 0.01 us  [shards(): weights = marks[:, :experts_all] + marks[:, experts_all:2 * experts_all]]
    unnamed x43 -> x53, local copies, waits for them, and re-layouts: 10.2 us -> 7.51 us
  transfers between devices with their start and end apart: 8 -> 1, of which waited for: 6 -> 0; matrix products, arithmetic and copies ran while one was open for 3% -> 4% of each run, Pallas kernels for 0% -> 0%
where the time goes in v2:
time: 145 us
  Pallas kernels  109 us (75%)
  matrix products  14.5 us (10%)
  local copies, waits for them, and re-layouts  13.7 us (9%)
  starting transfers between devices  4.89 us (3%)
  other arithmetic  2.96 us (2%)
    pallas_call x2, Pallas kernels, gather_sp(): pl.pallas_call(functools.partial(gather_kernel, spread, count // 2), out_...  57.5 us
    pallas_call x1, Pallas kernels, reduce_sp(): pl.pallas_call(functools.partial(reduce_sp_kernel, lines), out_shape=jax....  26.1 us
    pallas_call x1, Pallas kernels, mixer(): pl.pallas_call(functools.partial(joined_kernel, 'sp'), out_shape=shape((l...  11.5 us
    pallas_call x1, Pallas kernels, reduce_tp(): pl.pallas_call(reduce_tp_kernel, out_shape=jax.ShapeDtypeStruct(block, F3...  8.95 us
    unnamed x53, local copies, waits for them, and re-layouts  7.51 us
    dot_general x1, matrix products, shards(): result = result + weight * dot(hidden, routed_down_weight[e])  5.61 us
    dot_general x1, matrix products, shards(): lax.dot_general(hidden, shared_down, (((1,), (1,)), ((), ())), preferred_...  5.49 us
    ppermute x1, starting transfers between devices, mixer(): rim = lax.ppermute(tails, 'sp', [(k, k + 1) for k in range(count - 1)])  4.89 us
  transfers between devices with their start and end apart: 1, of which 0 were waited for; matrix products, arithmetic and copies ran while one was open for 4% of the time, Pallas kernels for 0%

profile of v2, /device:TPU:0, one launch (start us, length us, event | category | flops | bytes accessed | tf_op | source)
XLA Modules:
  0.0 145.0 jit_solution(4246198870779907049)
XLA Ops:
  0.0 0.0 copy-start
  0.0 0.8 slice.31
  0.8 0.7 slice.32
  1.5 0.7 slice.30
  2.2 4.9 %collective-permute-start = (bf16[8,2048]{1,0:T(8,128)(2,1)S(1)}, bf16[8,2048]{1,0:T(8,128)(2,1)S(1)}, u32[]{:S(2)}, u32[]{:S(2)}) collective-permute-start(bf16[8,2048]{1,0:T(8,128)(2,1)S(1)} %pad_maximum_fusion.1), channel_id=1, source_target_pairs={{0,4},{4,8},{8,12},{12,16},{16,20},{20,24},{24,28},{1,5},{5,9},{9,... | collective-permute-start | bytes 98312 | tf_op jit(solution)/shard_map/ppermute | solution.py:454
  7.1 0.7 select_reduce_fusion
  7.8 0.1 copy.40
  7.9 0.1 copy.41
  8.0 1.2 constant_dynamic-slice_fusion.2
  9.3 0.0 copy-start.23
  9.3 0.0 copy-start.20
  9.3 0.0 copy-start.21
  9.3 0.0 copy-start.8
  9.3 0.0 copy-start.9
  9.3 0.0 copy-start.10
  9.3 0.0 copy-start.11
  9.4 0.0 copy-start.12
  9.4 0.0 copy-start.13
  9.4 0.0 copy-start.14
  9.4 1.6 %constant_dynamic-slice_fusion = (bf16[2048,64]{1,0:T(8,128)(2,1)S(1)}, bf16[2048,64]{1,0:T(8,128)(2,1)S(1)}) fusion(bf16[2048,128]{1,0:T(8,128)(2,1)} %param.45, s32[]{:T(128)S(6)} %select_n.20, bf16[2048,128]{1,0:T(8,128)(2,1)} %param.44), kind=kLoop, calls=%fused_computation.46 | loop fusion | bytes 1048580 | tf_op jit(solution)/shard_map/dynamic_slice | solution.py:499
  11.0 0.5 pad_maximum_fusion.refs_1_
  11.6 0.6 subtract_convert_fusion
  12.2 0.7 copy.42
  12.9 0.0 copy-done.23
  12.9 0.1 broadcast_in_dim.30
  12.9 0.1 broadcast_in_dim_reshape.3.skip_ref
  13.0 0.0 copy-done.20
  13.0 0.1 copy.38.pre_ref
  13.1 0.0 copy-done.21
  13.1 0.1 copy.39.extra_ref
  13.2 0.0 collective-permute-done.rim_ref
  13.2 0.0 copy-done.8
  13.3 0.0 copy-done.9
  13.3 0.0 copy-done.10
  13.3 0.0 copy-done.11
  13.3 0.0 copy-done.12
  13.3 0.0 copy-done.13
  13.3 0.0 copy-done.14
  13.3 4.6 %shard_map.217 = (bf16[144,1024]{1,0:T(8,128)(2,1)S(1)}, f32[256,1024]{1,0:T(8,128)S(1)}, bf16[256,512]{1,0:T(8,128)(2,1)S(1)}, f32[256,16]{1,0:T(8,128)S(1)}) custom-call(bf16[256,1024]{1,0:T(8,128)(2,1)S(1)} %copy-done.8, bf16[256,512]{1,0:T(8,128)(2,1)S(1)} %copy-done.9, bf16[256,512]{1,0:T(8,128)(2,1)S(1)} %copy-done.10, ...), custom_call_target="tpu_custom_call" | custom-call | flops 1000000000 | bytes 4000000 | tf_op jit(solution)/shard_map/pallas_call | solution.py:456
  17.9 0.0 copy-start.6
  17.9 0.7 copy-done.6
  18.6 0.6 copy-done.7
  19.3 29.9 %shard_map.218 = (bf16[8,144,1024]{2,1,0:T(8,128)(2,1)S(1)}, bf16[2048,192]{1,0:T(8,128)(2,1)S(1)}) custom-call(bf16[144,1024]{1,0:T(8,128)(2,1)S(1)} %get-tuple-element.11.refs_0_, bf16[2048,192]{1,0:T(8,128)(2,1)S(1)} %pad_maximum_fusion.refs_1_), custom_call_target="tpu_custom_call" | custom-call | tf_op jit(solution)/shard_map/pallas_call | solution.py:258
  49.2 1.4 copy-done.3
  50.6 1.0 copy-done.5
  51.6 11.5 %shard_map.219 = bf16[256,2048]{1,0:T(8,128)(2,1)} custom-call(bf16[8,144,1024]{2,1,0:T(8,128)(2,1)} %copy-done.3, f32[256,1024]{1,0:T(8,128)} %copy-done.4, bf16[256,512]{1,0:T(8,128)(2,1)} %copy-done.6, f32[256,16]{1,0:T(8,128)} %copy-done.7, bf16[256,1024]{1,0:T(8,128)(2,1)} %gate_ref.1, f32[1,1024]{1,0:T(1,128)} %bitcast.25, bf16[1024,2048]{1,0:T(8,128)(2,1)} %out_w_ref.1), custom_call_target="tpu_custom_call" | custom-call | flops 1000000000 | bytes 9000000 | tf_op jit(solution)/shard_map/pallas_call | solution.py:482
  63.1 1.2 copy-done.2
  64.3 9.0 %shard_map.220 = f32[64,2048]{1,0:T(8,128)S(1)} custom-call(bf16[4,64,2048]{2,1,0:T(8,128)(2,1)S(1)} %bitcast.22), custom_call_target="tpu_custom_call" | custom-call | tf_op jit(solution)/shard_map/pallas_call | solution.py:425
  73.3 0.2 fusion.29
  73.5 0.1 fusion.31
  73.6 0.5 copy-done.15
  74.2 0.1 concatenate.11.refs_0_
  74.3 27.6 %shard_map.221 = bf16[8,64,2176]{2,1,0:T(8,128)(2,1)S(1)} custom-call(bf16[64,2176]{1,0:T(8,128)(2,1)S(1)} %concatenate.11.refs_0_), custom_call_target="tpu_custom_call" | custom-call | tf_op jit(solution)/shard_map/pallas_call | solution.py:258
  101.9 0.1 copy.44
  102.0 0.0 copy-start.24
  102.0 1.9 %fusion.6 = f32[512,64]{0,1:T(8,128)S(1)} fusion(bf16[512,2176]{1,0:T(8,128)(2,1)S(1)} %bitcast.17, bf16[2048,192]{1,0:T(8,128)(2,1)} %copy-done.5), kind=kOutput, calls=%fused_computation.7 | convolution fusion | flops 134217728 | bytes 2752512 | tf_op jit(solution)/shard_map/dot_general | solution.py:586
  103.9 0.0 copy-done.24
  103.9 1.5 %fusion.2 = f32[512,256]{1,0:T(8,128)} fusion(bf16[512,2176]{1,0:T(8,128)(2,1)S(1)} %bitcast.18, bf16[1,2048,256]{2,1,0:T(8,128)(2,1)S(1)} %copy-done.24), kind=kOutput, calls=%fused_computation.3 | convolution fusion | flops 536870912 | bytes 3670016 | tf_op jit(solution)/shard_map/dot_general | solution.py:593
  105.4 0.0 copy-done
  105.5 5.6 %fusion.15 = f32[512,2048]{1,0:T(8,128)} fusion(bf16[512,2176]{1,0:T(8,128)(2,1)S(1)} %bitcast.19, bf16[1,256,2048]{2,1,0:T(8,128)(2,1)S(1)} %copy-done, bf16[1,2048,256]{2,1,0:T(8,128)(2,1)} %param.41, f32[512,256]{1,0:T(8,128)} %fusion.2), kind=kOutput, calls=%fused_computation.11 | convolution fusion | flops 1074528256 | bytes 8912896 | tf_op jit(solution)/shard_map/dot_general | solution.py:595
  111.1 5.5 %add_convert_fusion = bf16[512,2048]{1,0:T(8,128)(2,1)} fusion(f32[512,2048]{1,0:T(8,128)} %fusion.15, f32[512]{0:T(512)S(1)} %bitcast.24, bf16[512,2176]{1,0:T(8,128)(2,1)S(1)} %bitcast.20, bf16[2048,192]{1,0:T(8,128)(2,1)} %copy-done.5, f32[512,64]{0,1:T(8,128)S(1)} %fusion.6), kind=kOutput, calls=%fused_computation | convolution fusion | flops 271777792 | bytes 9308160 | tf_op jit(solution)/shard_map/dot_general | solution.py:587
  116.6 1.6 %copy-done.1 = bf16[512,2048]{1,0:T(8,128)(2,1)S(1)} copy-done((bf16[512,2048]{1,0:T(8,128)(2,1)S(1)}, bf16[512,2048]{1,0:T(8,128)(2,1)}, u32[]{:S(2)}) %copy-start.1) | copy-done | bytes 2097176
  118.2 26.1 %shard_map.222 = bf16[64,2048]{1,0:T(8,128)(2,1)S(1)} custom-call(bf16[8,64,2048]{2,1,0:T(8,128)(2,1)S(1)} %bitcast.21), custom_call_target="tpu_custom_call" | custom-call | tf_op jit(solution)/shard_map/pallas_call | solution.py:360
  144.3 0.8 fusion.32
  (25 shorter events, 0.1 us)
Async XLA Ops:
  0.0 105.5 %copy-start = (bf16[1,256,2048]{2,1,0:T(8,128)(2,1)S(1)}, bf16[1,256,2048]{2,1,0:T(8,128)(2,1)}, u32[]{:S(2)}) copy-start(bf16[1,256,2048]{2,1,0:T(8,128)(2,1)} %param.42) | copy-start | bytes 3145732
  2.2 11.0 %collective-permute-start = (bf16[8,2048]{1,0:T(8,128)(2,1)S(1)}, bf16[8,2048]{1,0:T(8,128)(2,1)S(1)}, u32[]{:S(2)}, u32[]{:S(2)}) collective-permute-start(bf16[8,2048]{1,0:T(8,128)(2,1)S(1)} %pad_maximum_fusion.1), channel_id=1, source_target_pairs={{0,4},{4,8},{8,12},{12,16},{16,20},{20,24},{24,28},{1,5},{5,9},{9,... | collective-permute-start | bytes 98312 | tf_op jit(solution)/shard_map/ppermute | solution.py:454
  9.3 3.6 %copy-start.23 = (f32[16]{0:T(128)S(1)}, f32[16]{0:T(128)}, u32[]{:S(2)}) copy-start(f32[16]{0:T(128)} %param.34) | copy-start | bytes 196
  9.3 3.7 %copy-start.20 = (f32[256,16]{0,1:T(8,128)S(1)}, f32[256,16]{0,1:T(8,128)}, u32[]{:S(2)}) copy-start(f32[256,16]{0,1:T(8,128)} %param.28) | copy-start | bytes 49156
  9.3 3.8 %copy-start.21 = (f32[256,16]{0,1:T(8,128)S(1)}, f32[256,16]{0,1:T(8,128)}, u32[]{:S(2)}) copy-start(f32[256,16]{0,1:T(8,128)} %param.29) | copy-start | bytes 49156
  9.3 3.9 %copy-start.8 = (bf16[256,1024]{1,0:T(8,128)(2,1)S(1)}, bf16[256,1024]{1,0:T(8,128)(2,1)}, u32[]{:S(2)}) copy-start(bf16[256,1024]{1,0:T(8,128)(2,1)} %v_ref.1) | copy-start | bytes 1572868
  9.3 3.9 %copy-start.9 = (bf16[256,512]{1,0:T(8,128)(2,1)S(1)}, bf16[256,512]{1,0:T(8,128)(2,1)}, u32[]{:S(2)}) copy-start(bf16[256,512]{1,0:T(8,128)(2,1)} %b_ref.1) | copy-start | bytes 786436
  9.3 3.9 %copy-start.10 = (bf16[256,512]{1,0:T(8,128)(2,1)S(1)}, bf16[256,512]{1,0:T(8,128)(2,1)}, u32[]{:S(2)}) copy-start(bf16[256,512]{1,0:T(8,128)(2,1)} %c_ref.1) | copy-start | bytes 786436
  9.3 3.9 %copy-start.11 = (bf16[4,1024]{1,0:T(4,128)(2,1)S(1)}, bf16[4,1024]{1,0:T(4,128)(2,1)}, u32[]{:S(2)}) copy-start(bf16[4,1024]{1,0:T(4,128)(2,1)} %vk_ref.1) | copy-start | bytes 24580
  9.4 3.9 %copy-start.12 = (bf16[4,512]{1,0:T(4,128)(2,1)S(1)}, bf16[4,512]{1,0:T(4,128)(2,1)}, u32[]{:S(2)}) copy-start(bf16[4,512]{1,0:T(4,128)(2,1)} %bk_ref.1) | copy-start | bytes 12292
  9.4 3.9 %copy-start.13 = (bf16[4,512]{1,0:T(4,128)(2,1)S(1)}, bf16[4,512]{1,0:T(4,128)(2,1)}, u32[]{:S(2)}) copy-start(bf16[4,512]{1,0:T(4,128)(2,1)} %ck_ref.1) | copy-start | bytes 12292
  9.4 3.9 %copy-start.14 = (f32[16]{0:T(128)S(1)}, f32[16]{0:T(128)}, u32[]{:S(2)}) copy-start(f32[16]{0:T(128)} %param.33) | copy-start | bytes 196
  17.9 0.7 copy-start.6
  18.6 0.7 copy-start.7
  19.3 29.9 %copy-start.4 = (f32[256,1024]{1,0:T(8,128)}, f32[256,1024]{1,0:T(8,128)S(1)}, u32[]{:S(2)}) copy-start(f32[256,1024]{1,0:T(8,128)S(1)} %get-tuple-element.13.y_ref) | copy-start | bytes 3145732
  49.2 1.4 copy-start.3
  50.6 1.0 copy-start.5
  51.6 21.7 %copy-start.17 = (bf16[64,2048]{1,0:T(8,128)(2,1)S(1)}, bf16[64,2048]{1,0:T(8,128)(2,1)}, u32[]{:S(2)}) copy-start(bf16[64,2048]{1,0:T(8,128)(2,1)} %param.23) | copy-start | bytes 786436
  63.1 1.2 copy-start.2
  64.3 9.2 %copy-start.22 = (f32[2048]{0:T(1024)S(1)}, f32[2048]{0:T(1024)}, u32[]{:S(2)}) copy-start(f32[2048]{0:T(1024)} %param.37) | copy-start | bytes 24580
  64.3 9.9 %copy-start.18 = (bf16[64,8]{1,0:T(8,128)(2,1)S(1)}, bf16[64,8]{1,0:T(8,128)(2,1)}, u32[]{:S(2)}) copy-start(bf16[64,8]{1,0:T(8,128)(2,1)} %subtract_convert_fusion) | copy-start | bytes 3076
  64.3 9.9 %copy-start.19 = (bf16[64,8]{1,0:T(8,128)(2,1)S(1)}, bf16[64,8]{1,0:T(8,128)(2,1)}, u32[]{:S(2)}) copy-start(bf16[64,8]{1,0:T(8,128)(2,1)} %copy.42) | copy-start | bytes 3076
  73.5 0.7 copy-start.15
  102.0 1.9 %copy-start.24 = (bf16[1,2048,256]{2,1,0:T(8,128)(2,1)S(1)}, bf16[1,2048,256]{2,1,0:T(8,128)(2,1)}, u32[]{:S(2)}) copy-start(bf16[1,2048,256]{2,1,0:T(8,128)(2,1)} %param.40) | copy-start | bytes 3145732
  116.6 1.6 %copy-start.1 = (bf16[512,2048]{1,0:T(8,128)(2,1)S(1)}, bf16[512,2048]{1,0:T(8,128)(2,1)}, u32[]{:S(2)}) copy-start(bf16[512,2048]{1,0:T(8,128)(2,1)} %add_convert_fusion) | copy-start | bytes 6291460
  118.2 26.1 %copy-start.16 = (bf16[64,2048]{1,0:T(8,128)(2,1)S(1)}, bf16[64,2048]{1,0:T(8,128)(2,1)}, u32[]{:S(2)}) copy-start(bf16[64,2048]{1,0:T(8,128)(2,1)} %copy-done.15) | copy-start | bytes 786436

commit v3 on v2

--- a/solution.py
+++ b/solution.py
@@ -141,7 +141,7 @@
 
 
 MESH = pl.DeviceIdType.MESH
-CUTS = 2
+CUTS = 4
 
 
 def greet(peers):
@@ -153,6 +153,10 @@
     pl.semaphore_wait(barrier, sum(jnp.where(here, 1, 0) for here, _, _ in peers))
 
 
+def cuts_of(rows):
+    return next(cuts for cuts in (4, 3, 2, 1) if rows % (16 * cuts) == 0)
+
+
 def gather_kernel(spread, lines, *refs):
     if spread is None:
         x_ref, out_ref, sent, landed = refs
@@ -160,7 +164,8 @@
         x_ref, mine_ref, out_ref, slices_ref, sent, landed, spread_sent, spread_landed = refs
     me = lax.axis_index("sp")
     z, y = me // 2, me % 2
-    half = x_ref.shape[0] // CUTS
+    cuts = cuts_of(x_ref.shape[0])
+    half = x_ref.shape[0] // cuts
     always = me >= 0
     peers = [
         (always, me + 1 - 2 * y, "sp"), (z > 0, me - 2, "sp"), (z < lines - 1, me + 2, "sp")
@@ -183,7 +188,7 @@
             device_id_type=MESH,
         )
 
-    for cut in range(CUTS):
+    for cut in range(cuts):
         for way, (here, peer, _) in enumerate(peers[:3]):
             @pl.when(here)
             def _():
@@ -204,7 +209,7 @@
 
     out_ref[me] = x_ref[...]
     for turn in range(1, lines):
-        for cut in range(CUTS):
+        for cut in range(cuts):
             for step, onward in ((-1, 2), (1, 1)):
                 far = z + step * turn
                 block = far * 2 + y
@@ -219,9 +224,9 @@
                         send(block, cut, onward, peers[onward][1], False).start()
 
     for line in range(lines):
-        for cut in range(CUTS):
+        for cut in range(cuts):
             send(line * 2 + 1 - y, cut, 0, peers[0][1], False).wait_recv()
-    for cut in range(CUTS):
+    for cut in range(cuts):
         for line in range(lines):
             send(line * 2 + y, cut, 0, peers[0][1], False).wait_send()
 
@@ -246,9 +251,9 @@
 
 def gather_sp(x, number, mine=None, held=0):
     count, parts = lax.axis_size("sp"), lax.axis_size("tp")
-    shape = jax.ShapeDtypeStruct
+    shape, cuts = jax.ShapeDtypeStruct, cuts_of(x.shape[0])
     lands = [shape((count, *x.shape), x.dtype)]
-    sems = [pltpu.SemaphoreType.DMA((3, count, CUTS)), pltpu.SemaphoreType.DMA((count, CUTS))]
+    sems = [pltpu.SemaphoreType.DMA((3, count, cuts)), pltpu.SemaphoreType.DMA((count, cuts))]
     operands, spread = [x], None
     if mine is not None:
         spread = (mine.shape[1] // 3, held, parts)
@@ -441,6 +446,53 @@
 
 def small_mesh():
     return lax.axis_size("sp") in (4, 8) and lax.axis_size("tp") == 4
+
+
+def expert_kernel(tile, experts_all, rows_ref, slices_ref, gate_ref, up_ref, down_ref, out_ref):
+    local, features = gate_ref.shape[:2]
+    piece = slices_ref.shape[1] // 3
+    first = lax.axis_index("sp") * local
+    dot = functools.partial(jnp.dot, preferred_element_type=F32)
+
+    def chunk(number, _):
+        at = pl.ds(pl.multiple_of(number * tile, tile), tile)
+        rows = rows_ref[at, :features]
+        marks = rows_ref[at, features:].astype(F32)
+        lane = lax.broadcasted_iota(jnp.int32, marks.shape, 1)
+        both = dot(rows, slices_ref[:, : 2 * piece])
+        shared = (silu(both[:, :piece]) * both[:, piece:]).astype(BF16)
+        hidden = []
+        for e in range(local):
+            named = (lane == first + e) | (lane == first + e + experts_all)
+            weight = jnp.sum(jnp.where(named, marks, 0.0), axis=1, keepdims=True)
+            opened = (silu(dot(rows, gate_ref[e])) * dot(rows, up_ref[e])).astype(BF16)
+            hidden.append((opened, weight))
+        wide = 512
+        for begin in range(0, features, wide):
+            cols = slice(begin, begin + wide)
+            total = lax.dot_general(
+                shared, slices_ref[cols, 2 * piece :], (((1,), (1,)), ((), ())),
+                preferred_element_type=F32,
+            )
+            for e, (opened, weight) in enumerate(hidden):
+                total += weight * dot(opened, down_ref[e, :, cols])
+            out_ref[at, cols] = total.astype(BF16)
+        return 0
+
+    lax.fori_loop(0, rows_ref.shape[0] // tile, chunk, 0)
+
+
+def experts(rows, slices, gate, up, down, experts_all):
+    return pl.pallas_call(
+        functools.partial(expert_kernel, 256, experts_all),
+        out_shape=jax.ShapeDtypeStruct((rows.shape[0], gate.shape[1]), BF16),
+        in_specs=[VMEM] * 5,
+        out_specs=VMEM,
+        compiler_params=pltpu.CompilerParams(vmem_limit_bytes=56 << 20),
+        cost_estimate=pl.CostEstimate(
+            flops=2 * 10**9, bytes_accessed=8 * 10**6, transcendentals=10**5
+        ),
+    )(rows, slices, gate, up, down)
 
 
 def mixer(
@@ -546,10 +598,6 @@
         head_norm_gain, mixer_output_weight,
         (common_gate_weight, common_up_weight, common_down_weight),
     )
-    piece = slices.shape[1] // 3
-    shared_gate, shared_up, shared_down = (
-        slices[:, k * piece : (k + 1) * piece] for k in range(3)
-    )
     count = lax.axis_size("sp")
     local_experts = routed_gate_weight.shape[0]
     experts_all = local_experts * count
@@ -578,22 +626,9 @@
         gathered = gather_sp(packed, 3)[0].reshape(-1, packed.shape[1])
     else:
         gathered = lax.all_gather(packed, "sp", axis=0, tiled=True)
-    rows = gathered[:, :features]
-    marks = gathered[:, features:].astype(F32)
-    weights = marks[:, :experts_all] + marks[:, experts_all : 2 * experts_all]
-    first = lax.axis_index("sp") * local_experts
-    dot = functools.partial(jnp.dot, preferred_element_type=F32)
-    hidden = (jax.nn.silu(dot(rows, shared_gate)) * dot(rows, shared_up)).astype(BF16)
-    result = lax.dot_general(
-        hidden, shared_down, (((1,), (1,)), ((), ())), preferred_element_type=F32
-    )
-    for e in range(local_experts):
-        weight = lax.dynamic_slice_in_dim(weights, first + e, 1, axis=1)
-        hidden = (
-            jax.nn.silu(dot(rows, routed_gate_weight[e])) * dot(rows, routed_up_weight[e])
-        ).astype(BF16)
-        result = result + weight * dot(hidden, routed_down_weight[e])
-    result = result.astype(BF16)
+    result = experts(
+        gathered, slices, routed_gate_weight, routed_up_weight, routed_down_weight, experts_all
+    )
     if small_mesh():
         added = reduce_sp(result.reshape(count, row_count, features), 4)
     else:

time: 145 us -> 138 us (0.952)
  matrix products: 14.5 us -> 0 us
  Pallas kernels: 109 us -> 117 us
    dot_general x4 -> x0, matrix products: 14.5 us -> none  [the longest x1 5.61 us: shards(): result = result + weight * dot(hidden, routed_down_weight[e])]
    pallas_call x0 -> x1, Pallas kernels: none -> 7.43 us  [experts(): pl.pallas_call(functools.partial(expert_kernel, 256, experts_all), out_sh...]
    unnamed x53 -> x44, local copies, waits for them, and re-layouts: 7.51 us -> 8.12 us
  transfers between devices with their start and end apart: 1 -> 1, of which waited for: 0 -> 0; matrix products, arithmetic and copies ran while one was open for 4% -> 3% of each run, Pallas kernels for 0% -> 0%
where the time goes in v3:
time: 138 us; the launch traced here: 137 us
  Pallas kernels  117 us (85%)
  local copies, waits for them, and re-layouts  12.7 us (9%)
  starting transfers between devices  4.89 us (4%)
  other arithmetic  2.35 us (2%)
    pallas_call x2, Pallas kernels, gather_sp(): pl.pallas_call(functools.partial(gather_kernel, spread, count // 2), out_...  58.4 us
    pallas_call x1, Pallas kernels, reduce_sp(): pl.pallas_call(functools.partial(reduce_sp_kernel, lines), out_shape=jax....  26.4 us
    pallas_call x1, Pallas kernels, mixer(): pl.pallas_call(functools.partial(joined_kernel, 'sp'), out_shape=shape((l...  11.5 us
    pallas_call x1, Pallas kernels, reduce_tp(): pl.pallas_call(reduce_tp_kernel, out_shape=jax.ShapeDtypeStruct(block, F3...  8.95 us
    unnamed x44, local copies, waits for them, and re-layouts  8.12 us
    pallas_call x1, Pallas kernels, experts(): pl.pallas_call(functools.partial(expert_kernel, 256, experts_all), out_sh...  7.43 us
    ppermute x1, starting transfers between devices, mixer(): rim = lax.ppermute(tails, 'sp', [(k, k + 1) for k in range(count - 1)])  4.89 us
    pallas_call x1, Pallas kernels, mixer(): pl.pallas_call(local_kernel, out_shape=(shape((STATE + 16, width), BF16),...  4.62 us
  transfers between devices with their start and end apart: 1, of which 0 were waited for; matrix products, arithmetic and copies ran while one was open for 3% of the time, Pallas kernels for 0%

profile of v3, /device:TPU:0, one launch (start us, length us, event | category | flops | bytes accessed | tf_op | source)
XLA Modules:
  0.0 137.5 jit_solution(10004961242391169520)
XLA Ops:
  0.0 0.0 copy-start
  0.0 0.8 slice.9
  0.8 0.7 slice.10
  1.5 0.7 slice.11
  2.2 4.9 %collective-permute-start = (bf16[8,2048]{1,0:T(8,128)(2,1)S(1)}, bf16[8,2048]{1,0:T(8,128)(2,1)S(1)}, u32[]{:S(2)}, u32[]{:S(2)}) collective-permute-start(bf16[8,2048]{1,0:T(8,128)(2,1)S(1)} %pad_maximum_fusion.1), channel_id=1, source_target_pairs={{0,4},{4,8},{8,12},{12,16},{16,20},{20,24},{24,28},{1,5},{5,9},{9,... | collective-permute-start | bytes 98312 | tf_op jit(solution)/shard_map/ppermute | solution.py:506
  7.1 0.7 select_reduce_fusion
  7.8 0.1 copy.34
  7.9 0.1 copy.35
  8.0 0.0 copy-done
  8.0 0.2 constant_dynamic-slice_fusion.2
  8.2 0.0 copy-start.17
  8.2 0.0 copy-start.18
  8.2 0.0 copy-start.20
  8.2 0.0 copy-start.9
  8.2 0.0 copy-start.10
  8.3 0.0 copy-start.11
  8.3 0.0 copy-start.12
  8.3 0.0 copy-start.13
  8.3 0.0 copy-start.14
  8.3 0.0 copy-start.15
  8.3 1.6 %constant_dynamic-slice_fusion = (bf16[2048,64]{1,0:T(8,128)(2,1)S(1)}, bf16[2048,64]{1,0:T(8,128)(2,1)S(1)}) fusion(bf16[2048,128]{1,0:T(8,128)(2,1)} %param.45, s32[]{:T(128)S(6)} %select_n.17, bf16[2048,128]{1,0:T(8,128)(2,1)} %param.44), kind=kLoop, calls=%fused_computation.13 | loop fusion | bytes 1048580 | tf_op jit(solution)/shard_map/dynamic_slice | solution.py:551
  10.0 0.5 pad_maximum_fusion.refs_1_
  10.5 0.1 copy.36
  10.6 0.0 copy-done.17
  10.6 0.1 copy.32.pre_ref
  10.7 0.0 copy-done.18
  10.7 0.1 copy.33.extra_ref
  10.8 0.0 copy-done.20
  10.8 0.1 broadcast_in_dim.30
  10.9 0.1 broadcast_in_dim_reshape.3.skip_ref
  11.0 0.0 collective-permute-done.rim_ref
  11.0 0.0 copy-done.9
  11.0 0.0 copy-done.10
  11.0 0.0 copy-done.11
  11.0 0.0 copy-done.12
  11.0 0.0 copy-done.13
  11.0 0.0 copy-done.14
  11.0 0.0 copy-done.15
  11.1 4.6 %shard_map.217 = (bf16[144,1024]{1,0:T(8,128)(2,1)S(1)}, f32[256,1024]{1,0:T(8,128)S(1)}, bf16[256,512]{1,0:T(8,128)(2,1)S(1)}, f32[256,16]{1,0:T(8,128)S(1)}) custom-call(bf16[256,1024]{1,0:T(8,128)(2,1)S(1)} %copy-done.9, bf16[256,512]{1,0:T(8,128)(2,1)S(1)} %copy-done.10, bf16[256,512]{1,0:T(8,128)(2,1)S(1)} %copy-done.11, ...), custom_call_target="tpu_custom_call" | custom-call | flops 1000000000 | bytes 4000000 | tf_op jit(solution)/shard_map/pallas_call | solution.py:508
  15.7 0.0 copy-start.7
  15.7 0.7 copy-done.7
  16.4 0.0 copy-start.8
  16.4 0.6 copy-done.8
  17.0 0.0 copy-start.5
  17.0 30.2 %shard_map.218 = (bf16[8,144,1024]{2,1,0:T(8,128)(2,1)S(1)}, bf16[2048,192]{1,0:T(8,128)(2,1)S(1)}) custom-call(bf16[144,1024]{1,0:T(8,128)(2,1)S(1)} %get-tuple-element.11.refs_0_, bf16[2048,192]{1,0:T(8,128)(2,1)S(1)} %pad_maximum_fusion.refs_1_), custom_call_target="tpu_custom_call" | custom-call | tf_op jit(solution)/shard_map/pallas_call | solution.py:263
  47.2 0.0 copy-done.5
  47.2 0.0 copy-start.4
  47.2 1.4 copy-done.4
  48.6 1.0 copy-done.6
  49.6 11.5 %shard_map.219 = bf16[256,2048]{1,0:T(8,128)(2,1)} custom-call(bf16[8,144,1024]{2,1,0:T(8,128)(2,1)} %copy-done.4, f32[256,1024]{1,0:T(8,128)} %copy-done.5, bf16[256,512]{1,0:T(8,128)(2,1)} %copy-done.7, f32[256,16]{1,0:T(8,128)} %copy-done.8, bf16[256,1024]{1,0:T(8,128)(2,1)} %gate_ref.2, f32[1,1024]{1,0:T(1,128)} %bitcast.9, bf16[1024,2048]{1,0:T(8,128)(2,1)} %out_w_ref.1), custom_call_target="tpu_custom_call" | custom-call | flops 1000000000 | bytes 9000000 | tf_op jit(solution)/shard_map/pallas_call | solution.py:534
  61.1 1.2 copy-done.3
  62.3 9.0 %shard_map.220 = f32[64,2048]{1,0:T(8,128)S(1)} custom-call(bf16[4,64,2048]{2,1,0:T(8,128)(2,1)S(1)} %bitcast.7), custom_call_target="tpu_custom_call" | custom-call | tf_op jit(solution)/shard_map/pallas_call | solution.py:430
  71.3 0.0 copy-done.16
  71.3 0.2 fusion
  71.5 0.0 copy-done.19
  71.5 0.1 fusion.2
  71.6 0.1 concatenate.11.refs_0_
  71.7 28.2 %shard_map.221 = bf16[8,64,2176]{2,1,0:T(8,128)(2,1)S(1)} custom-call(bf16[64,2176]{1,0:T(8,128)(2,1)S(1)} %concatenate.11.refs_0_), custom_call_target="tpu_custom_call" | custom-call | tf_op jit(solution)/shard_map/pallas_call | solution.py:263
  99.9 0.0 copy-start.1
  99.9 1.3 copy-done.1
  101.3 7.4 %shard_map.222 = bf16[512,2048]{1,0:T(8,128)(2,1)} custom-call(bf16[512,2176]{1,0:T(8,128)(2,1)} %bitcast.5, bf16[2048,192]{1,0:T(8,128)(2,1)} %copy-done.6, bf16[1,2048,256]{2,1,0:T(8,128)(2,1)} %gate_ref.3, bf16[1,2048,256]{2,1,0:T(8,128)(2,1)} %up_ref.1, bf16[1,256,2048]{2,1,0:T(8,128)(2,1)} %down_ref.1), custom_call_target="tpu_custom_call" | custom-call | flops 2000000000 | bytes 8000000 | tf_op jit(solution)/shard_map/pallas_call | solution.py:486
  108.7 1.6 %copy-done.2 = bf16[512,2048]{1,0:T(8,128)(2,1)S(1)} copy-done((bf16[512,2048]{1,0:T(8,128)(2,1)S(1)}, bf16[512,2048]{1,0:T(8,128)(2,1)}, u32[]{:S(2)}) %copy-start.2) | copy-done | bytes 2097176
  110.3 26.4 %shard_map.223 = bf16[64,2048]{1,0:T(8,128)(2,1)S(1)} custom-call(bf16[8,64,2048]{2,1,0:T(8,128)(2,1)S(1)} %bitcast.6), custom_call_target="tpu_custom_call" | custom-call | tf_op jit(solution)/shard_map/pallas_call | solution.py:365
  136.7 0.8 fusion.3
  (10 shorter events, 0.0 us)
Async XLA Ops:
  0.0 8.0 %copy-start = (bf16[2048,128]{1,0:T(8,128)(2,1)S(1)}, bf16[2048,128]{1,0:T(8,128)(2,1)}, u32[]{:S(2)}) copy-start(bf16[2048,128]{1,0:T(8,128)(2,1)} %param.43) | copy-start | bytes 1572868
  2.2 8.8 %collective-permute-start = (bf16[8,2048]{1,0:T(8,128)(2,1)S(1)}, bf16[8,2048]{1,0:T(8,128)(2,1)S(1)}, u32[]{:S(2)}, u32[]{:S(2)}) collective-permute-start(bf16[8,2048]{1,0:T(8,128)(2,1)S(1)} %pad_maximum_fusion.1), channel_id=1, source_target_pairs={{0,4},{4,8},{8,12},{12,16},{16,20},{20,24},{24,28},{1,5},{5,9},{9,... | collective-permute-start | bytes 98312 | tf_op jit(solution)/shard_map/ppermute | solution.py:506
  8.2 2.4 %copy-start.17 = (f32[256,16]{0,1:T(8,128)S(1)}, f32[256,16]{0,1:T(8,128)}, u32[]{:S(2)}) copy-start(f32[256,16]{0,1:T(8,128)} %param.28) | copy-start | bytes 49156
  8.2 2.5 %copy-start.18 = (f32[256,16]{0,1:T(8,128)S(1)}, f32[256,16]{0,1:T(8,128)}, u32[]{:S(2)}) copy-start(f32[256,16]{0,1:T(8,128)} %param.29) | copy-start | bytes 49156
  8.2 2.6 %copy-start.20 = (f32[16]{0:T(128)S(1)}, f32[16]{0:T(128)}, u32[]{:S(2)}) copy-start(f32[16]{0:T(128)} %param.34) | copy-start | bytes 196
  8.2 2.8 %copy-start.9 = (bf16[256,1024]{1,0:T(8,128)(2,1)S(1)}, bf16[256,1024]{1,0:T(8,128)(2,1)}, u32[]{:S(2)}) copy-start(bf16[256,1024]{1,0:T(8,128)(2,1)} %v_ref.1) | copy-start | bytes 1572868
  8.2 2.7 %copy-start.10 = (bf16[256,512]{1,0:T(8,128)(2,1)S(1)}, bf16[256,512]{1,0:T(8,128)(2,1)}, u32[]{:S(2)}) copy-start(bf16[256,512]{1,0:T(8,128)(2,1)} %b_ref.1) | copy-start | bytes 786436
  8.3 2.7 %copy-start.11 = (bf16[256,512]{1,0:T(8,128)(2,1)S(1)}, bf16[256,512]{1,0:T(8,128)(2,1)}, u32[]{:S(2)}) copy-start(bf16[256,512]{1,0:T(8,128)(2,1)} %c_ref.1) | copy-start | bytes 786436
  8.3 2.7 %copy-start.12 = (bf16[4,1024]{1,0:T(4,128)(2,1)S(1)}, bf16[4,1024]{1,0:T(4,128)(2,1)}, u32[]{:S(2)}) copy-start(bf16[4,1024]{1,0:T(4,128)(2,1)} %vk_ref.1) | copy-start | bytes 24580
  8.3 2.7 %copy-start.13 = (bf16[4,512]{1,0:T(4,128)(2,1)S(1)}, bf16[4,512]{1,0:T(4,128)(2,1)}, u32[]{:S(2)}) copy-start(bf16[4,512]{1,0:T(4,128)(2,1)} %bk_ref.1) | copy-start | bytes 12292
  8.3 2.7 %copy-start.14 = (bf16[4,512]{1,0:T(4,128)(2,1)S(1)}, bf16[4,512]{1,0:T(4,128)(2,1)}, u32[]{:S(2)}) copy-start(bf16[4,512]{1,0:T(4,128)(2,1)} %ck_ref.1) | copy-start | bytes 12292
  8.3 2.7 %copy-start.15 = (f32[16]{0:T(128)S(1)}, f32[16]{0:T(128)}, u32[]{:S(2)}) copy-start(f32[16]{0:T(128)} %param.33) | copy-start | bytes 196
  15.7 0.7 copy-start.7
  16.4 0.6 copy-start.8
  17.0 30.2 %copy-start.5 = (f32[256,1024]{1,0:T(8,128)}, f32[256,1024]{1,0:T(8,128)S(1)}, u32[]{:S(2)}) copy-start(f32[256,1024]{1,0:T(8,128)S(1)} %get-tuple-element.13.y_ref) | copy-start | bytes 3145732
  47.2 1.4 %copy-start.4 = (bf16[8,144,1024]{2,1,0:T(8,128)(2,1)}, bf16[8,144,1024]{2,1,0:T(8,128)(2,1)S(1)}, u32[]{:S(2)}) copy-start(bf16[8,144,1024]{2,1,0:T(8,128)(2,1)S(1)} %get-tuple-element.12.states_ref) | copy-start | bytes 7077892
  48.6 1.0 copy-start.6
  49.6 21.7 %copy-start.16 = (bf16[64,2048]{1,0:T(8,128)(2,1)S(1)}, bf16[64,2048]{1,0:T(8,128)(2,1)}, u32[]{:S(2)}) copy-start(bf16[64,2048]{1,0:T(8,128)(2,1)} %param.23) | copy-start | bytes 786436
  61.1 1.2 copy-start.3
  62.3 9.2 %copy-start.19 = (f32[2048]{0:T(1024)S(1)}, f32[2048]{0:T(1024)}, u32[]{:S(2)}) copy-start(f32[2048]{0:T(1024)} %param.37) | copy-start | bytes 24580
  99.9 1.3 copy-start.1
  108.7 1.6 %copy-start.2 = (bf16[512,2048]{1,0:T(8,128)(2,1)S(1)}, bf16[512,2048]{1,0:T(8,128)(2,1)}, u32[]{:S(2)}) copy-start(bf16[512,2048]{1,0:T(8,128)(2,1)} %shard_map.222) | copy-start | bytes 6291460
